TPU v7x, 32 devices: a whole 2x2x4 slice. The times are simulated.
32 devices in a mesh: sp: 8 (over z, y), tp: 4 (over x, core).
Axes of the slice: x: 2, y: 2, z: 4, core: 2. Of those that a mesh axis runs over, the one named last changes fastest.
Arguments:
- mixer_input: bfloat16 [2048, 2048], P('sp', 'tp'), may hold values from -6 to 6
- step_log: float32 [2048, 128], P('sp'), may hold values from -4.21 to -1.89
- forget_log: float32 [2048, 128], P('sp'), may hold values from -0.7 to 0
- decay_rate: float32 [128, 64], replicated, may hold values from 0 to 0.8
- frequency: float32 [128, 64], replicated, may hold values from 1 to 64
- input_map: float32 [2, 128, 64, 16], P(None, 'tp'), may hold values from -2.5 to 2.5
- output_map: float32 [2, 128, 16, 64], P(None, 'tp'), may hold values from -1.25 to 1.25
- skip_gain: float32 [2048], replicated, may hold values from -3 to 3
- value_weight: bfloat16 [2048, 2048], replicated, may hold values from -0.125 to 0.125
- gate_weight: bfloat16 [2048, 2048], replicated, may hold values from -0.125 to 0.125
- residual: bfloat16 [2048, 2048], P(('sp', 'tp')), may hold values from -6 to 6
- norm_gain: bfloat16 [2048], replicated, may hold values from 0.099609375 to 1.8984375
- ffn_gate: bfloat16 [2048, 5632], P('sp', 'tp'), may hold values from -0.125 to 0.125
- ffn_up: bfloat16 [2048, 5632], P('sp', 'tp'), may hold values from -0.125 to 0.125
- conv_taps: float32 [3, 5632], replicated, may hold values from -6 to 6
- ffn_down: bfloat16 [5632, 2048], P('tp', 'sp'), may hold values from -0.078125 to 0.078125
Outputs:
- updated: bfloat16 [2048, 2048], P(('sp', 'tp'))
All inputs are finite; a program needn't handle non-finite values.
Results may differ from a plain program's by a relative error of at most 0.014.
Values may be sent and summed in bfloat16 or wider, within the bound.
A program may use at most 192 MiB of HBM per device.

v0:
```python
import jax
import jax.numpy as jnp
from jax import lax
from jax.sharding import PartitionSpec as P


def entering(value, axis, join, neutral):
    count, mine = (lax.axis_size(axis), lax.axis_index(axis))
    pieces = jax.tree.map(lambda part: lax.all_gather(part, axis), value)
    running = jax.tree.map(
        lambda part, zero: jnp.full_like(part, 0) + jnp.asarray(zero, part.dtype), value, neutral
    )

    def hop(position, running):
        longer = join(running, jax.tree.map(lambda part: part[position], pieces))
        return jax.tree.map(lambda new, old: jnp.where(position < mine, new, old), longer, running)

    return lax.fori_loop(0, count - 1, hop, running)


def shifted_2(block, axis, distance):
    devices = range(lax.axis_size(axis))
    route = [(i - distance, i) for i in devices if i - distance in devices]
    return lax.ppermute(block, axis, route)


def compose(earlier, later):
    decay_real = later[0] * earlier[0] - later[1] * earlier[1]
    decay_imag = later[0] * earlier[1] + later[1] * earlier[0]
    state_real = later[0] * earlier[2] - later[1] * earlier[3] + later[2]
    state_imag = later[0] * earlier[3] + later[1] * earlier[2] + later[3]
    return (decay_real, decay_imag, state_real, state_imag)


def local(
    mixer_input,
    step_log,
    forget_log,
    decay_rate,
    frequency,
    input_map,
    output_map,
    skip_gain,
    value_weight,
    gate_weight,
    residual,
    norm_gain,
    ffn_gate,
    ffn_up,
    conv_taps,
    ffn_down,
):
    tp_index = lax.axis_index("tp")
    positions, local_width = mixer_input.shape
    entries = input_map.shape[2]
    channels = input_map.shape[3]
    groups = local_width // channels
    flat = groups * entries
    first_group = tp_index * groups
    real_part = -lax.dynamic_slice_in_dim(decay_rate, first_group, groups, 0)[None]
    omega = lax.dynamic_slice_in_dim(frequency, first_group, groups, 0)[None]
    steps = jnp.exp(lax.dynamic_slice_in_dim(step_log, first_group, groups, 1))[:, :, None]
    retained = jnp.exp(lax.dynamic_slice_in_dim(forget_log, first_group, groups, 1))[:, :, None]
    divisor = real_part * real_part + omega * omega
    magnitude = jnp.exp(real_part * steps)
    angle = omega * steps
    held_real = magnitude * jnp.cos(angle)
    held_imag = magnitude * jnp.sin(angle)
    factor_real = ((held_real - 1.0) * real_part + held_imag * omega) / divisor
    factor_imag = (held_imag * real_part - (held_real - 1.0) * omega) / divisor
    decay_real = (retained * held_real).reshape(positions, flat)
    decay_imag = (retained * held_imag).reshape(positions, flat)
    signal = mixer_input.astype(jnp.float32)
    grouped = signal.reshape(positions, groups, channels)
    mapped_real = jnp.einsum("tgh,gph->tgp", grouped, input_map[0], precision=lax.Precision.HIGHEST)
    mapped_imag = jnp.einsum("tgh,gph->tgp", grouped, input_map[1], precision=lax.Precision.HIGHEST)
    drive_real = (factor_real * mapped_real - factor_imag * mapped_imag).reshape(positions, flat)
    drive_imag = (factor_real * mapped_imag + factor_imag * mapped_real).reshape(positions, flat)
    span = 32
    blocks = positions // span
    pieces = tuple(
        (
            array.reshape(blocks, span, flat)
            for array in (decay_real, decay_imag, drive_real, drive_imag)
        )
    )
    inner = lax.associative_scan(compose, pieces, axis=1)
    block_ends = tuple((array[:, -1] for array in inner))
    through = lax.associative_scan(compose, block_ends, axis=0)
    summary = tuple((array[-1] for array in through))
    identity = (
        jnp.ones((flat,), jnp.float32),
        jnp.zeros((flat,), jnp.float32),
        jnp.zeros((flat,), jnp.float32),
        jnp.zeros((flat,), jnp.float32),
    )
    before = entering(summary, "sp", compose, identity)
    shifted = tuple(
        (
            jnp.concatenate([neutral[None], array[:-1]], axis=0)
            for neutral, array in zip(identity, through)
        )
    )
    opening = compose(before, shifted)
    start_real = opening[2][:, None]
    start_imag = opening[3][:, None]
    state_real = inner[2] + inner[0] * start_real - inner[1] * start_imag
    state_imag = inner[3] + inner[0] * start_imag + inner[1] * start_real
    response = (
        jnp.einsum(
            "tgp,ghp->tgh",
            state_real.reshape(positions, groups, entries),
            output_map[0],
            precision=lax.Precision.HIGHEST,
        )
        - jnp.einsum(
            "tgp,ghp->tgh",
            state_imag.reshape(positions, groups, entries),
            output_map[1],
            precision=lax.Precision.HIGHEST,
        )
    ).reshape(positions, local_width)
    skip_local = lax.dynamic_slice_in_dim(skip_gain, tp_index * local_width, local_width, 0)
    response = response + skip_local * signal
    activated = jax.nn.gelu(response).astype(jnp.bfloat16)
    tp_count = lax.axis_size("tp")
    own_rows = positions // tp_count
    row_block = lax.all_to_all(
        activated.reshape(tp_count, own_rows, local_width),
        "tp",
        split_axis=0,
        concat_axis=2,
        tiled=True,
    )[0]
    value = jnp.dot(row_block, value_weight, preferred_element_type=jnp.float32)
    gate = jnp.dot(row_block, gate_weight, preferred_element_type=jnp.float32)
    mixed = value * jax.nn.sigmoid(gate)
    stream = (residual.astype(jnp.float32) + mixed).astype(jnp.bfloat16)
    stream_wide = stream.astype(jnp.float32)
    scale = lax.rsqrt(jnp.mean(stream_wide * stream_wide, axis=1, keepdims=True) + 1e-06)
    normed = (stream_wide * scale * norm_gain.astype(jnp.float32)).astype(jnp.bfloat16)
    hidden_width = ffn_gate.shape[1]
    whole_rows = lax.all_gather(normed, "tp", axis=0, tiled=True)
    gate_pre = jnp.dot(
        whole_rows,
        lax.all_gather(ffn_gate, "sp", axis=0, tiled=True),
        preferred_element_type=jnp.float32,
    )
    up_pre = jnp.dot(
        whole_rows,
        lax.all_gather(ffn_up, "sp", axis=0, tiled=True),
        preferred_element_type=jnp.float32,
    )
    history = conv_taps.shape[0] - 1
    boundary = shifted_2(gate_pre[positions - history :], "sp", 1)
    extended = jnp.concatenate([boundary, gate_pre], axis=0)
    tap_weights = lax.dynamic_slice_in_dim(conv_taps, tp_index * hidden_width, hidden_width, 1)
    conv_gate = tap_weights[0] * extended[0:positions]
    for offset in range(1, history + 1):
        conv_gate = conv_gate + tap_weights[offset] * extended[offset : offset + positions]
    hidden = (jax.nn.silu(conv_gate) * up_pre).astype(jnp.bfloat16)
    partial_value = jnp.dot(
        hidden,
        lax.all_gather(ffn_down, "sp", axis=1, tiled=True),
        preferred_element_type=jnp.float32,
    )
    ffn_out = lax.psum_scatter(
        partial_value.astype(jnp.bfloat16), "tp", scatter_dimension=0, tiled=True
    ).astype(jnp.float32)
    return (stream_wide + ffn_out).astype(jnp.bfloat16)


def solution(mesh):
    in_specs = (
        P("sp", "tp"),
        P("sp", None),
        P("sp", None),
        P(),
        P(),
        P(None, "tp", None, None),
        P(None, "tp", None, None),
        P(),
        P(),
        P(),
        P(("sp", "tp"), None),
        P(),
        P("sp", "tp"),
        P("sp", "tp"),
        P(),
        P("tp", "sp"),
    )
    out_specs = P(("sp", "tp"), None)
    return jax.shard_map(local, mesh=mesh, in_specs=in_specs, out_specs=out_specs, check_vma=False)
```

profile of v0, /device:TPU:0, one launch (start us, length us, event | category | flops | bytes accessed | tf_op | source)
XLA Modules:
  0.0 838.9 jit_solution(10226663767159143703)
XLA Ops:
  12.2 12.6 %fusion.15 = (f32[256,32,64]{0,2,1:T(8,128)}, f32[256,32,64]{0,2,1:T(8,128)S(1)}) fusion(f32[32,64,256]{2,1,0:T(8,128)S(1)} %fusion.41, f32[32,64]{1,0:T(8,128)S(1)} %get-tuple-element.278, f32[32,64]{1,0:T(8,128)S(1)} %copy.143, f32[256,32]{0,1:T(8,128)S(1)} %exp.20, f32[32,64]{1,0:T(8,128)S(1)} %get-tuple-element.277, ...), kind=kOutput, calls=%fused_computation.28 | convolution fusion | flops 110624768 | bytes 6897664 | tf_op jit(solution)/shard_map/tgh,gph->tgp/dot_general | solution.py:76
  71.8 10.7 %multiply_multiply_fusion.1 = (f32[8,32,2048]{2,0,1:T(8,128)S(1)}, f32[8,32,2048]{2,0,1:T(8,128)S(1)}) fusion(f32[8,32,2048]{2,1,0:T(8,128)} %mul.650, f32[8,32,2048]{2,1,0:T(8,128)} %mul.653, f32[2048]{0:T(1024)S(1)} %mul.655, f32[2048]{0:T(1024)S(1)} %mul.651), kind=kLoop, calls=%fused_computation.35 | loop fusion | flops 3145728 | bytes 8404992 | tf_op jit(solution)/shard_map/mul | solution.py:71
  214.3 10.3 %pad.241 = f32[8,32,2048]{2,0,1:T(8,128)} pad(f32[8,16,2048]{2,0,1:T(8,128)} %add.583, f32[]{:T(128)} %constant.56.clone.1), padding=0_0_0x1_0_1x0_0_0 | pad | bytes 3145732 | tf_op jit(solution)/shard_map/pad | solution.py:87
  227.0 10.2 %pad.240 = f32[8,32,2048]{2,0,1:T(8,128)} pad(f32[8,16,2048]{2,0,1:T(8,128)} %pad_maximum_fusion.3, f32[]{:T(128)} %constant.56.clone.1), padding=0_0_0x0_1_1x0_0_0 | pad | bytes 3145732 | tf_op jit(solution)/shard_map/pad | solution.py:87
  238.1 6.5 pad.239
  245.9 6.4 pad.238
  281.3 6.4 pad.220
  287.8 6.4 pad.221
  296.5 6.4 pad.255
  303.1 6.5 pad.254
  315.8 32.4 %all-gather = f32[8,1,2048]{2,1,0:T(1,128)S(1)} all-gather(f32[1,1,2048]{2,1,0:T(1,128)S(1)} %add_bitcast_fusion.11), channel_id=1, replica_groups=mesh['sp'=8,'tp'=4] {'sp'}, dimensions={0}, use_global_device_ids=true | all-gather | bytes 73728 | tf_op jit(solution)/shard_map/all_gather | solution.py:9
  348.3 30.5 %all-gather.1 = f32[8,1,2048]{2,1,0:T(1,128)S(1)} all-gather(f32[1,1,2048]{2,1,0:T(1,128)S(1)} %add_bitcast_fusion.8), channel_id=1, replica_groups=mesh['sp'=8,'tp'=4] {'sp'}, dimensions={0}, use_global_device_ids=true | all-gather | bytes 73728 | tf_op jit(solution)/shard_map/all_gather | solution.py:9
  378.9 30.5 %all-gather.2 = f32[8,1,2048]{2,1,0:T(1,128)S(1)} all-gather(f32[1,1,2048]{2,1,0:T(1,128)S(1)} %add_bitcast_fusion.6), channel_id=1, replica_groups=mesh['sp'=8,'tp'=4] {'sp'}, dimensions={0}, use_global_device_ids=true | all-gather | bytes 73728 | tf_op jit(solution)/shard_map/all_gather | solution.py:9
  409.5 30.5 %all-gather.3 = f32[8,1,2048]{2,1,0:T(1,128)S(1)} all-gather(f32[1,1,2048]{2,1,0:T(1,128)S(1)} %add_bitcast_fusion.4), channel_id=1, replica_groups=mesh['sp'=8,'tp'=4] {'sp'}, dimensions={0}, use_global_device_ids=true | all-gather | bytes 73728 | tf_op jit(solution)/shard_map/all_gather | solution.py:9
  440.8 8.6 %multiply_subtract_fusion = (f32[8,32,2048]{2,0,1:T(8,128)}, f32[8,32,2048]{2,0,1:T(8,128)S(1)}) fusion(f32[8,32,2048]{2,0,1:T(8,128)} %pad.220, f32[8,32,2048]{2,0,1:T(8,128)} %pad.221, f32[8,2048]{1,0:T(8,128)S(1)} %get-tuple-element.250, f32[8,2048]{1,0:T(8,128)S(1)} %get-tuple-element.249, f32[8,32,2048]{2,0,1:T(8,128)} %pad.240, ...), kind=kLoop, calls=%fused_computation.33 | loop fusion | flops 6291456 | bytes 21102592 | tf_op jit(solution)/shard_map/sub | solution.py:107
  464.5 7.3 fusion
  471.8 6.1 fusion.22
  483.4 5.9 all-to-all-done
  502.7 14.7 %all-gather.9.cloned.1.call-done = bf16[256,2048]{1,0:T(8,128)(2,1)} async-done(((bf16[64,2048]{1,0:T(8,128)(2,1)}), bf16[256,2048]{1,0:T(8,128)(2,1)}) %all-gather.9.cloned.1.call-update) | async-done | bytes 1048592 | tf_op jit(solution)/shard_map/all_gather | solution.py:143
  517.4 94.5 %all-gather.11.cloned.1.call-done = bf16[2048,1408]{1,0:T(8,128)(2,1)} async-done(((bf16[256,1408]{1,0:T(8,128)(2,1)}), bf16[2048,1408]{1,0:T(8,128)(2,1)}) %all-gather.11.cloned.1.call-update) | async-done | bytes 5767184 | tf_op jit(solution)/shard_map/all_gather | solution.py:146
  620.4 84.9 %all-gather.15.cloned.1.call-done = bf16[1408,2048]{1,0:T(8,128)(2,1)} async-done(((bf16[1408,256]{1,0:T(8,128)(2,1)}), bf16[1408,2048]{1,0:T(8,128)(2,1)}) %all-gather.15.cloned.1.call-update) | async-done | bytes 5767184 | tf_op jit(solution)/shard_map/all_gather | solution.py:164
  705.3 92.6 %all-gather.13.cloned.1.call-done = bf16[2048,1408]{1,0:T(8,128)(2,1)} async-done(((bf16[256,1408]{1,0:T(8,128)(2,1)}), bf16[2048,1408]{1,0:T(8,128)(2,1)}) %all-gather.13.cloned.1.call-update) | async-done | bytes 5767184 | tf_op jit(solution)/shard_map/all_gather | solution.py:151
  797.9 9.1 %convolution_convert_fusion = bf16[256,2048]{1,0:T(8,128)(2,1)} fusion(bf16[1408,2048]{1,0:T(8,128)(2,1)} %all-gather.15.cloned.1.call-done, bf16[256,2048]{1,0:T(8,128)(2,1)S(1)} %copy-done.47, bf16[2048,1408]{1,0:T(8,128)(2,1)} %all-gather.13.cloned.1.call-done, f32[256,1408]{1,0:T(8,128)S(1)} %fusion.59, f32[2,1408]{1,0:T(2,128)S(1)} %collective-permute-done, ...), kind=kOutput, calls=%fused_computation.14 | convolution fusion | flops 2958000128 | bytes 15101440 | tf_op jit(solution)/shard_map/dot_general | solution.py:162
  807.1 23.2 %reduce-scatter.2.cloned.1.call-done = bf16[64,2048]{1,0:T(8,128)(2,1)} async-done(((bf16[256,2048]{1,0:T(8,128)(2,1)}), bf16[64,2048]{1,0:T(8,128)(2,1)}) %reduce-scatter.2.cloned.1.call-update) | async-done | bytes 262160 | tf_op jit(solution)/shard_map/reduce_scatter | solution.py:167
  (350 shorter events, 271.1 us)
Async XLA Ops:
  71.8 10.7 %copy-start.22 = (f32[8,16,2048]{2,1,0:T(8,128)S(1)}, f32[8,16,2048]{2,1,0:T(8,128)}, u32[]{:S(2)}) copy-start(f32[8,16,2048]{2,1,0:T(8,128)} %slice.538) | copy-start | bytes 3145732
  71.8 10.7 %copy-start.23 = (f32[8,16,2048]{2,1,0:T(8,128)S(1)}, f32[8,16,2048]{2,1,0:T(8,128)}, u32[]{:S(2)}) copy-start(f32[8,16,2048]{2,1,0:T(8,128)} %slice.529) | copy-start | bytes 3145732
  71.8 10.7 %copy-start.24 = (f32[8,16,2048]{2,1,0:T(8,128)S(1)}, f32[8,16,2048]{2,1,0:T(8,128)}, u32[]{:S(2)}) copy-start(f32[8,16,2048]{2,1,0:T(8,128)} %slice.527) | copy-start | bytes 3145732
  71.8 10.7 %copy-start.25 = (f32[8,16,2048]{2,1,0:T(8,128)S(1)}, f32[8,16,2048]{2,1,0:T(8,128)}, u32[]{:S(2)}) copy-start(f32[8,16,2048]{2,1,0:T(8,128)} %slice.530) | copy-start | bytes 3145732
  103.7 7.8 copy-start.44
  158.0 10.0 %copy-start.43 = (f32[8,1,2048]{2,0,1:T(8,128)S(1)}, f32[8,1,2048]{2,0,1:T(8,128)}, u32[]{:S(2)}) copy-start(f32[8,1,2048]{2,0,1:T(8,128)} %slice.719) | copy-start | bytes 196612
  245.9 13.2 %copy-start.40 = (f32[8,1,2048]{2,0,1:T(8,128)S(1)}, f32[8,1,2048]{2,0,1:T(8,128)}, u32[]{:S(2)}) copy-start(f32[8,1,2048]{2,0,1:T(8,128)} %slice.685) | copy-start | bytes 196612
  252.3 6.8 copy-start.35
  259.1 7.1 copy-start.41
  262.7 11.1 %copy-start.42 = (f32[8,1,2048]{2,1,0:T(1,128)S(1)}, f32[8,1,2048]{2,1,0:T(1,128)}, u32[]{:S(2)}) copy-start(f32[8,1,2048]{2,1,0:T(1,128)} %slice.684) | copy-start | bytes 196612
  281.3 6.5 copy-start.26
  287.8 7.3 copy-start.6
  295.3 7.7 copy-start.27
  303.0 9.1 %copy-start.12 = (f32[8,32,2048]{2,0,1:T(8,128)S(1)}, f32[8,32,2048]{2,0,1:T(8,128)}, u32[]{:S(2)}) copy-start(f32[8,32,2048]{2,0,1:T(8,128)} %pad.241) | copy-start | bytes 6291460
  464.5 7.3 copy-start.1
  471.8 7.1 copy-start.36
  479.9 9.4 %all-to-all-start = ((bf16[4,64,512]{2,1,0:T(8,128)(2,1)}), bf16[4,64,512]{2,1,0:T(8,128)(2,1)S(1)}, u32[]{:S(2)}, u32[]{:S(2)}) async-start(bf16[4,64,512]{2,1,0:T(8,128)(2,1)} %bitcast.21), calls=%async_computation | async-start | bytes 524288 | tf_op jit(solution)/shard_map/all_to_all | solution.py:128
  483.3 34.1 %all-gather.9.cloned.1.call-start = ((), (), s32[]{:S(2)}) async-start(), calls=%async_computation.2 | async-start | bytes 1310720 | tf_op jit(solution)/shard_map/all_gather | solution.py:143
  500.6 111.3 %all-gather.11.cloned.1.call-start = ((), (), s32[]{:S(2)}) async-start(), calls=%async_computation.3 | async-start | bytes 6488064 | tf_op jit(solution)/shard_map/all_gather | solution.py:146
  501.4 204.0 %all-gather.15.cloned.1.call-start = ((), (), s32[]{:S(2)}) async-start(), calls=%async_computation.5 | async-start | bytes 6488064 | tf_op jit(solution)/shard_map/all_gather | solution.py:164
  502.1 295.8 %all-gather.13.cloned.1.call-start = ((), (), s32[]{:S(2)}) async-start(), calls=%async_computation.4 | async-start | bytes 6488064 | tf_op jit(solution)/shard_map/all_gather | solution.py:151
  502.7 327.6 %reduce-scatter.2.cloned.1.call-start = ((), (), s32[]{:S(2)}) async-start(), calls=%async_computation.6 | async-start | bytes 1310720 | tf_op jit(solution)/shard_map/reduce_scatter | solution.py:167
  517.4 280.5 %copy-start.47 = (bf16[256,2048]{1,0:T(8,128)(2,1)S(1)}, bf16[256,2048]{1,0:T(8,128)(2,1)}, u32[]{:S(2)}) copy-start(bf16[256,2048]{1,0:T(8,128)(2,1)} %all-gather.9.cloned.1.call-done) | copy-start | bytes 3145732
  616.7 181.2 %collective-permute-start = (f32[2,1408]{1,0:T(2,128)S(1)}, f32[2,1408]{1,0:T(2,128)S(1)}, u32[]{:S(2)}, u32[]{:S(2)}) collective-permute-start(f32[2,1408]{1,0:T(2,128)S(1)} %slice.800), channel_id=1, source_target_pairs={{0,4},{4,8},{8,12},{12,16},{16,20},{20,24},{24,28},{1,5},{5,9},{9,... | collective-permute-start | bytes 33800 | tf_op jit(solution)/shard_map/ppermute | solution.py:24
  (31 other events, 101.2 us)
Sparse Core Ops, SparseCore 0:
  500.7 16.6 all-gather.8
  519.6 92.2 all-gather.10
  614.0 91.2 all-gather.14
  707.4 90.4 all-gather.12
  807.2 22.9 reduce-scatter.1
where the time goes:
time: 853 us; the launch traced here: 839 us
  waiting for transfers between devices  318 us (37%)
  local copies, waits for them, and re-layouts  231 us (27%)
  blocking collectives  124 us (15%)
  other arithmetic  93.3 us (11%)
  matrix products  52.1 us (6%)
  between operations  14.7 us (2%)
    pad x32, local copies, waits for them, and re-layouts, local(): inner = lax.associative_scan(compose, pieces, axis=1)  140 us
    all_gather x4, blocking collectives, entering(): pieces = jax.tree.map(lambda part: lax.all_gather(part, axis), value)  124 us
    all_gather x1, waiting for transfers between devices, local(): lax.all_gather(ffn_gate, 'sp', axis=0, tiled=True)  94.5 us
    all_gather x1, waiting for transfers between devices, local(): lax.all_gather(ffn_up, 'sp', axis=0, tiled=True)  92.6 us
    all_gather x1, waiting for transfers between devices, local(): lax.all_gather(ffn_down, 'sp', axis=1, tiled=True)  84.9 us
    slice x21, local copies, waits for them, and re-layouts, local(): inner = lax.associative_scan(compose, pieces, axis=1)  33.3 us
    reduce_scatter x1, waiting for transfers between devices, local(): lax.psum_scatter(partial_value.astype(jnp.bfloat16), 'tp', scatter_dimens...  23.2 us
    add x16, other arithmetic, local(): inner = lax.associative_scan(compose, pieces, axis=1)  19.5 us
  transfers between devices with their start and end apart: 7, of which 6 were waited for; matrix products, arithmetic and copies ran while one was open for 1% of the time, Pallas kernels for 0%

commit v1 on v0

v1 whole, which is shorter than its diff:
```python
import functools
import math

import jax
import jax.numpy as jnp
from jax import lax
from jax.experimental import pallas as pl
from jax.experimental.pallas import tpu as pltpu
from jax.sharding import PartitionSpec as P

LANES = 128
SEGMENTS = 8
CHUNK = 64


def sin_cos(angle):
    turns = jnp.floor(angle * (1.0 / math.pi) + 0.5)
    r = angle - turns * 3.140625
    r = r - turns * 9.67025756835937500e-4
    r = r - turns * 6.278329571113e-7
    half = turns * 0.5
    sign = 1.0 - 4.0 * (half - jnp.floor(half))
    q = r * r
    s = -2.3889859e-08
    for c in (2.7525562e-06, -1.9840874e-04, 8.3333310e-03, -1.6666667e-01):
        s = s * q + c
    s = r + r * (q * s)
    c_ = 2.0875723e-09
    for c in (-2.7557314e-07, 2.4801587e-05, -1.3888889e-03, 4.1666667e-02, -0.5):
        c_ = c_ * q + c
    c_ = 1.0 + q * c_
    return sign * s, sign * c_


def ssm_kernel(
    n_sp, groups, per_tile, tiles_per_block,
    x_ref, step_ref, forget_ref, rate_ref, w_in_ref, w_out_ref, skip_ref, out_ref,
    steps, kept, pr, pi, sr, si, fin, excl, summary, slots, before, packed, resp,
    send_sem, recv_sem,
):
    me = lax.axis_index("sp")
    first = lax.axis_index("tp") * groups
    rows = x_ref.shape[0]
    tiles = w_in_ref.shape[0]
    span = rows // SEGMENTS
    width = step_ref.shape[1]
    entries = LANES // per_tile

    if n_sp > 1:
        barrier = pltpu.get_barrier_semaphore()
        for d in range(1, n_sp):
            pl.semaphore_signal(
                barrier, inc=1, device_id={"sp": lax.rem(me + d, n_sp)},
                device_id_type=pl.DeviceIdType.MESH,
            )

    steps[...] = jnp.exp(step_ref[...])
    kept[...] = jnp.exp(forget_ref[...])

    def spread(array, shape):
        lane = lax.broadcasted_iota(jnp.int32, shape, 1)
        result = jnp.broadcast_to(array[:, 0:1], shape)
        for j in range(1, per_tile):
            result = jnp.where(lane < j * entries, result, array[:, j : j + 1])
        return result

    def tile(k, carry):
        block = pl.multiple_of((k // tiles_per_block) * LANES, LANES)
        shift = lax.rem(2 * width - (first + per_tile * k), width)
        a_real = rate_ref[0, pl.ds(k, 1), :]
        omega = rate_ref[1, pl.ds(k, 1), :]
        c_real = rate_ref[2, pl.ds(k, 1), :]
        c_imag = rate_ref[3, pl.ds(k, 1), :]
        for start in range(0, rows, CHUNK):
            at = pl.ds(start, CHUNK)
            shape = (CHUNK, LANES)
            step = spread(pltpu.roll(steps[at, :], shift, 1), shape)
            keep = spread(pltpu.roll(kept[at, :], shift, 1), shape)
            magnitude = jnp.exp(a_real * step)
            sine, cosine = sin_cos(omega * step)
            held_real = magnitude * cosine
            held_imag = magnitude * sine
            pr[k, at, :] = keep * held_real
            pi[k, at, :] = keep * held_imag
            less = held_real - 1.0
            factor_real = less * c_real + held_imag * c_imag
            factor_imag = held_imag * c_real - less * c_imag
            mapped = jnp.dot(
                x_ref[at, pl.ds(block, LANES)], w_in_ref[k],
                preferred_element_type=jnp.float32,
            )
            m_real, m_imag = mapped[:, :LANES], mapped[:, LANES:]
            sr[k, at, :] = factor_real * m_real - factor_imag * m_imag
            si[k, at, :] = factor_real * m_imag + factor_imag * m_real
        at = pl.ds(0, SEGMENTS, stride=span)
        p_r, p_i = pr[k, at, :], pi[k, at, :]
        s_r, s_i = sr[k, at, :], si[k, at, :]
        for j in range(1, span):
            at = pl.ds(j, SEGMENTS, stride=span)
            a_r, a_i = pr[k, at, :], pi[k, at, :]
            s_r, s_i = (
                a_r * s_r - a_i * s_i + sr[k, at, :],
                a_r * s_i + a_i * s_r + si[k, at, :],
            )
            p_r, p_i = a_r * p_r - a_i * p_i, a_r * p_i + a_i * p_r
            pr[k, at, :] = p_r
            pi[k, at, :] = p_i
            sr[k, at, :] = s_r
            si[k, at, :] = s_i
        for c, value in enumerate((p_r, p_i, s_r, s_i)):
            fin[c] = value
        t_r = jnp.ones((1, LANES), jnp.float32)
        t_i = jnp.zeros((1, LANES), jnp.float32)
        u_r, u_i = t_i, t_i
        for s in range(SEGMENTS):
            for c, value in enumerate((t_r, t_i, u_r, u_i)):
                excl[c, k, pl.ds(s, 1), :] = value
            a_r, a_i = fin[0, pl.ds(s, 1), :], fin[1, pl.ds(s, 1), :]
            b_r, b_i = fin[2, pl.ds(s, 1), :], fin[3, pl.ds(s, 1), :]
            t_r, t_i = a_r * t_r - a_i * t_i, a_r * t_i + a_i * t_r
            u_r, u_i = a_r * u_r - a_i * u_i + b_r, a_r * u_i + a_i * u_r + b_i
        for c, value in enumerate((t_r, t_i, u_r, u_i)):
            summary[c, pl.ds(k, 1), :] = value
        return carry

    lax.fori_loop(0, tiles, tile, 0)

    def copy(d):
        return pltpu.make_async_remote_copy(
            src_ref=summary, dst_ref=slots.at[d - 1],
            send_sem=send_sem.at[d - 1], recv_sem=recv_sem.at[d - 1],
            device_id={"sp": lax.rem(me + d, n_sp)},
            device_id_type=pl.DeviceIdType.MESH,
        )

    before[...] = jnp.zeros_like(before)
    if n_sp > 1:
        pl.semaphore_wait(barrier, n_sp - 1)
        for d in range(1, n_sp):
            @pl.when(me + d < n_sp)
            def _():
                copy(d).start()

    for start in range(0, resp.shape[1], LANES):
        at = pl.ds(start, LANES)
        resp[:, at] = skip_ref[:, at] * x_ref[:, at].astype(jnp.float32)

    for d in range(n_sp - 1, 0, -1):
        @pl.when(me >= d)
        def _():
            copy(d).wait_recv()
            a_r, a_i = slots[d - 1, 0], slots[d - 1, 1]
            h_r, h_i = before[0], before[1]
            before[0] = a_r * h_r - a_i * h_i + slots[d - 1, 2]
            before[1] = a_r * h_i + a_i * h_r + slots[d - 1, 3]

    def finish(k, carry):
        block = pl.multiple_of((k // tiles_per_block) * LANES, LANES)
        h_r, h_i = before[0, pl.ds(k, 1), :], before[1, pl.ds(k, 1), :]
        t_r, t_i = excl[0, k], excl[1, k]
        o_r = t_r * h_r - t_i * h_i + excl[2, k]
        o_i = t_r * h_i + t_i * h_r + excl[3, k]
        for s in range(SEGMENTS):
            at = pl.ds(s * span, span)
            b_r, b_i = o_r[s : s + 1, :], o_i[s : s + 1, :]
            a_r, a_i = pr[k, at, :], pi[k, at, :]
            packed[at, :LANES] = (sr[k, at, :] + a_r * b_r - a_i * b_i).astype(jnp.bfloat16)
            packed[at, LANES:] = (si[k, at, :] + a_r * b_i + a_i * b_r).astype(jnp.bfloat16)
        resp[:, pl.ds(block, LANES)] += jnp.dot(
            packed[...], w_out_ref[k], preferred_element_type=jnp.float32
        )
        return carry

    lax.fori_loop(0, tiles, finish, 0)
    for start in range(0, resp.shape[1], LANES):
        at = pl.ds(start, LANES)
        out_ref[:, at] = jax.nn.gelu(resp[:, at]).astype(out_ref.dtype)
    for d in range(1, n_sp):
        @pl.when(me + d < n_sp)
        def _():
            copy(d).wait_send()


def state_space(n_sp, x, step_log, forget_log, rate, freq, in_map, out_map, skip):
    rows, local_width = x.shape
    _, groups, entries, channels = in_map.shape
    per_tile = LANES // entries
    tiles = groups // per_tile
    per_block = LANES // channels
    tiles_per_block = per_block // per_tile
    a_real = -rate.reshape(tiles, LANES)
    omega = freq.reshape(tiles, LANES)
    divisor = a_real * a_real + omega * omega
    rates = jnp.stack([a_real, omega, a_real / divisor, omega / divisor])
    slot = jnp.arange(per_block)[None, :, None]
    own = per_tile * (jnp.arange(tiles) % tiles_per_block)
    mask = slot == own[:, None, None] + jnp.arange(per_tile)[None, None, :]
    w_in = in_map.astype(jnp.bfloat16).reshape(2, tiles, per_tile, entries, channels).transpose(1, 4, 0, 2, 3)
    w_in = jnp.where(mask[:, :, None, None, :, None], w_in[:, None], 0).reshape(tiles, LANES, 2 * LANES)
    sign = jnp.array([1.0, -1.0], jnp.float32)[:, None, None, None]
    w_out = (out_map * sign).astype(jnp.bfloat16).reshape(2, tiles, per_tile, channels, entries)
    w_out = w_out.transpose(1, 0, 2, 4, 3)[:, :, :, :, None, :]
    w_out = jnp.where(mask.transpose(0, 2, 1)[:, None, :, None, :, None], w_out, 0)
    w_out = w_out.reshape(tiles, 2 * LANES, LANES)
    vmem = pl.BlockSpec(memory_space=pltpu.VMEM)
    f32 = jnp.float32
    peers = max(n_sp - 1, 1)
    big = pltpu.VMEM((tiles, rows, LANES), f32)
    return pl.pallas_call(
        functools.partial(ssm_kernel, n_sp, groups, per_tile, tiles_per_block),
        out_shape=jax.ShapeDtypeStruct((rows, local_width), jnp.bfloat16),
        in_specs=[vmem] * 7,
        out_specs=vmem,
        scratch_shapes=[
            pltpu.VMEM(step_log.shape, f32), pltpu.VMEM(step_log.shape, f32),
            big, big, big, big,
            pltpu.VMEM((4, SEGMENTS, LANES), f32),
            pltpu.VMEM((4, tiles, SEGMENTS, LANES), f32),
            pltpu.VMEM((4, tiles, LANES), f32),
            pltpu.VMEM((peers, 4, tiles, LANES), f32),
            pltpu.VMEM((2, tiles, LANES), f32),
            pltpu.VMEM((rows, 2 * LANES), jnp.bfloat16),
            pltpu.VMEM((rows, local_width), f32),
            pltpu.SemaphoreType.DMA((peers,)),
            pltpu.SemaphoreType.DMA((peers,)),
        ],
        compiler_params=pltpu.CompilerParams(
            collective_id=0, has_side_effects=True, vmem_limit_bytes=40 * 2**20,
        ),
        cost_estimate=pl.CostEstimate(
            flops=60_000_000_000, bytes_accessed=4_000_000, transcendentals=0
        ),
    )(x, step_log, forget_log, rates, w_in, w_out, skip)


def ring_tables(n):
    if n % 2:
        return list(range(n))
    return list(range(0, n, 2)) + list(range(n - 1, 0, -2))


def ring_owner(n, position):
    if n % 2:
        return position
    return jnp.where(position < n // 2, 2 * position, 2 * (n - 1 - position) + 1)


def ring_position(n, index):
    if n % 2:
        return index
    return jnp.where(index % 2 == 0, index // 2, n - 1 - index // 2)


def ring_steps(n, block, direction):
    order = ring_tables(n)
    route = [(order[i], order[(i + direction) % n]) for i in range(n)]
    place = ring_position(n, lax.axis_index("sp"))
    for step in range(n):
        owner = ring_owner(n, lax.rem(place - direction * step + n * n, n))
        yield block, owner
        if step < n - 1:
            block = lax.ppermute(block, "sp", route)


def shifted_2(block, axis, distance):
    devices = range(lax.axis_size(axis))
    route = [(i - distance, i) for i in devices if i - distance in devices]
    return lax.ppermute(block, axis, route)


def local(
    mixer_input, step_log, forget_log, decay_rate, frequency, input_map, output_map,
    skip_gain, value_weight, gate_weight, residual, norm_gain, ffn_gate, ffn_up,
    conv_taps, ffn_down,
):
    tp_index = lax.axis_index("tp")
    n_sp = lax.axis_size("sp")
    tp_count = lax.axis_size("tp")
    positions, local_width = mixer_input.shape
    groups = input_map.shape[1]
    model = ffn_gate.shape[0] * n_sp
    hidden_width = ffn_gate.shape[1]

    gate_full = jnp.zeros((model, hidden_width), ffn_gate.dtype)
    up_full = jnp.zeros((model, hidden_width), ffn_up.dtype)
    depth = ffn_gate.shape[0]
    for block, owner in ring_steps(n_sp, ffn_gate, 1):
        gate_full = lax.dynamic_update_slice(gate_full, block, (owner * depth, 0))
        last_gate = block
    for block, owner in ring_steps(n_sp, ffn_up, -1):
        up_full = lax.dynamic_update_slice(up_full, block, (owner * depth, 0))
        last_up = block
    half = hidden_width // 2
    top, bottom = ffn_down[:half], ffn_down[half:]
    top, bottom, last_gate, last_up = lax.optimization_barrier((top, bottom, last_gate, last_up))
    down_full = jnp.zeros((hidden_width, model), ffn_down.dtype)
    wide = ffn_down.shape[1]
    for block, owner in ring_steps(n_sp, top, 1):
        down_full = lax.dynamic_update_slice(down_full, block, (0, owner * wide))
    for block, owner in ring_steps(n_sp, bottom, -1):
        down_full = lax.dynamic_update_slice(down_full, block, (half, owner * wide))

    activated = state_space(
        n_sp, mixer_input, step_log, forget_log,
        lax.dynamic_slice_in_dim(decay_rate, tp_index * groups, groups, 0),
        lax.dynamic_slice_in_dim(frequency, tp_index * groups, groups, 0),
        input_map, output_map,
        lax.dynamic_slice_in_dim(skip_gain, tp_index * local_width, local_width, 0)[None],
    )
    own_rows = positions // tp_count
    row_block = lax.all_to_all(
        activated.reshape(tp_count, own_rows, local_width),
        "tp", split_axis=0, concat_axis=2, tiled=True,
    )[0]
    value = jnp.dot(row_block, value_weight, preferred_element_type=jnp.float32)
    gate = jnp.dot(row_block, gate_weight, preferred_element_type=jnp.float32)
    mixed = value * jax.nn.sigmoid(gate)
    stream = (residual.astype(jnp.float32) + mixed).astype(jnp.bfloat16)
    stream_wide = stream.astype(jnp.float32)
    scale = lax.rsqrt(jnp.mean(stream_wide * stream_wide, axis=1, keepdims=True) + 1e-06)
    normed = (stream_wide * scale * norm_gain.astype(jnp.float32)).astype(jnp.bfloat16)
    whole_rows = lax.all_gather(normed, "tp", axis=0, tiled=True)
    gate_pre = jnp.dot(whole_rows, gate_full, preferred_element_type=jnp.float32)
    up_pre = jnp.dot(whole_rows, up_full, preferred_element_type=jnp.float32)
    history = conv_taps.shape[0] - 1
    boundary = shifted_2(gate_pre[positions - history :], "sp", 1)
    extended = jnp.concatenate([boundary, gate_pre], axis=0)
    tap_weights = lax.dynamic_slice_in_dim(conv_taps, tp_index * hidden_width, hidden_width, 1)
    conv_gate = tap_weights[0] * extended[0:positions]
    for offset in range(1, history + 1):
        conv_gate = conv_gate + tap_weights[offset] * extended[offset : offset + positions]
    hidden = (jax.nn.silu(conv_gate) * up_pre).astype(jnp.bfloat16)
    partial_value = jnp.dot(hidden, down_full, preferred_element_type=jnp.float32)
    ffn_out = lax.psum_scatter(
        partial_value.astype(jnp.bfloat16), "tp", scatter_dimension=0, tiled=True
    ).astype(jnp.float32)
    return (stream_wide + ffn_out).astype(jnp.bfloat16)


def solution(mesh):
    in_specs = (
        P("sp", "tp"), P("sp", None), P("sp", None), P(), P(),
        P(None, "tp", None, None), P(None, "tp", None, None),
        P(), P(), P(), P(("sp", "tp"), None), P(),
        P("sp", "tp"), P("sp", "tp"), P(), P("tp", "sp"),
    )
    out_specs = P(("sp", "tp"), None)
    return jax.shard_map(local, mesh=mesh, in_specs=in_specs, out_specs=out_specs, check_vma=False)
```

time: 853 us -> 271 us (0.32); the launches traced: 839 us -> 270 us
  waiting for transfers between devices: 318 us -> 96.2 us
  local copies, waits for them, and re-layouts: 231 us -> 60.7 us
  blocking collectives: 124 us -> 0 us
  other arithmetic: 93.3 us -> 9.34 us
  starting transfers between devices: 6.31 us -> 40.8 us
  matrix products: 52.1 us -> 25.8 us
  Pallas kernels: 0 us -> 23.2 us
    all_gather x3 -> x0, waiting for transfers between devices: 272 us -> none  [the longest x1 94.5 us: local(): lax.all_gather(ffn_gate, 'sp', axis=0, tiled=True)]
    pad x46 -> x0, local copies, waits for them, and re-layouts: 140 us -> none  [the longest x32 140 us: local(): inner = lax.associative_scan(compose, pieces, axis=1)]
    all_gather x4 -> x0, blocking collectives: 124 us -> none  [entering(): pieces = jax.tree.map(lambda part: lax.all_gather(part, axis), value)]
    ppermute x0 -> x28, waiting for transfers between devices: none -> 70.3 us  [ring_steps(): block = lax.ppermute(block, 'sp', route)]
    dynamic_update_slice x0 -> x32, local copies, waits for them, and re-layouts: none -> 39.6 us  [the longest x8 13 us: local(): up_full = lax.dynamic_update_slice(up_full, block, (owner * depth, 0))]
    add x45 -> x1, other arithmetic: 38.5 us -> 0.07 us  [state_space(): mask = slot == own[:, None, None] + jnp.arange(per_tile)[None, None, :]]
    slice x47 -> x1, local copies, waits for them, and re-layouts: 34 us -> 0.05 us  [local(): top, bottom = (ffn_down[:half], ffn_down[half:])]
    ppermute x0 -> x28, starting transfers between devices: none -> 33.1 us  [ring_steps(): block = lax.ppermute(block, 'sp', route)]
  transfers between devices with their start and end apart: 7 -> 32, of which waited for: 6 -> 19; matrix products, arithmetic and copies ran while one was open for 1% -> 31% of each run, Pallas kernels for 0% -> 9%
where the time goes in v1:
time: 271 us; the launch traced here: 270 us
  waiting for transfers between devices  96.2 us (35%)
  local copies, waits for them, and re-layouts  60.7 us (22%)
  starting transfers between devices  40.8 us (15%)
  matrix products  25.8 us (10%)
  Pallas kernels  23.2 us (9%)
  between operations  14.1 us (5%)
  other arithmetic  9.34 us (3%)
    ppermute x28, waiting for transfers between devices, ring_steps(): block = lax.ppermute(block, 'sp', route)  70.3 us
    ppermute x28, starting transfers between devices, ring_steps(): block = lax.ppermute(block, 'sp', route)  33.1 us
    reduce_scatter x1, waiting for transfers between devices, local(): lax.psum_scatter(partial_value.astype(jnp.bfloat16), 'tp', scatter_dimens...  25.9 us
    pallas_call x1, Pallas kernels, state_space(): pl.pallas_call(functools.partial(ssm_kernel, n_sp, groups, per_tile, tile...  23.2 us
    dynamic_update_slice x8, local copies, waits for them, and re-layouts, local(): up_full = lax.dynamic_update_slice(up_full, block, (owner * depth, 0))  13 us
    dynamic_update_slice x8, local copies, waits for them, and re-layouts, local(): gate_full = lax.dynamic_update_slice(gate_full, block, (owner * depth, 0))  11.8 us
    dot_general x1, matrix products, local(): jnp.dot(hidden, down_full, preferred_element_type=jnp.float32)  10.9 us
    dynamic_update_slice x8, local copies, waits for them, and re-layouts, local(): down_full = lax.dynamic_update_slice(down_full, block, (0, owner * wide))  8.43 us
  transfers between devices with their start and end apart: 32, of which 19 were waited for; matrix products, arithmetic and copies ran while one was open for 31% of the time, Pallas kernels for 9%

profile of v1, /device:TPU:0, one launch (start us, length us, event | category | flops | bytes accessed | tf_op | source)
XLA Modules:
  0.0 270.2 jit_solution(15508737628594840809)
XLA Ops:
  6.5 3.0 %collective-permute-start.8 = (bf16[256,1408]{1,0:T(8,128)(2,1)}, bf16[256,1408]{1,0:T(8,128)(2,1)}, u32[]{:S(2)}, u32[]{:S(2)}) collective-permute-start(bf16[256,1408]{1,0:T(8,128)(2,1)} %param.30), channel_id=1, source_target_pairs={{0,4},{8,0},{16,8},{24,16},{28,24},{20,28},{12,20},{4,12},{1,5},{9... | collective-permute-start | bytes 2162696 | tf_op jit(solution)/shard_map/ppermute | solution.py:262
  19.1 2.9 %broadcast_select_fusion.1 = bf16[16,8,16,2,2,64]{5,4,3,2,1,0:T(2,128)(2,1)} fusion(pred[16,8,2]{2,1,0:T(8,128)(4,1)S(1)} %iota_compare_fusion.1, bf16[16,16,2,2,64]{4,3,2,1,0:T(2,128)(2,1)S(1)} %copy.39), kind=kLoop, calls=%fused_computation.1 | loop fusion | flops 524288 | bytes 1179904 | tf_op jit(solution)/shard_map/jit(_where)/select_n | solution.py:199
  22.0 4.4 %select_n.195.w_in_ref = bf16[16,128,256]{2,1,0:T(8,128)(2,1)S(1)} reshape(bf16[16,8,16,2,2,64]{5,4,3,2,1,0:T(2,128)(2,1)} %broadcast_select_fusion.1) | data formatting | bytes 2097152 | tf_op jit(solution)/shard_map/jit(_where)/select_n | solution.py:199
  29.4 23.2 %shard_map.163 = bf16[256,512]{1,0:T(8,128)(2,1)} custom-call(bf16[256,512]{1,0:T(8,128)(2,1)S(1)} %copy-done, f32[256,128]{1,0:T(8,128)S(1)} %copy-done.1, f32[256,128]{1,0:T(8,128)S(1)} %copy-done.2, f32[4,16,128]{2,1,0:T(8,128)S(1)} %pad_maximum_fusion.1.rate_ref, bf16[16,128,256]{2,1,0:T(8,128)(2,1)S(1)} %select_n.195.w_in_ref, ...), custom_call_target="tpu_custom_call" | custom-call | flops 60000002048 | bytes 4000000 | tf_op jit(solution)/shard_map/pallas_call | solution.py:209
  52.6 3.5 %all-to-all-start = ((bf16[4,64,512]{2,1,0:T(8,128)(2,1)}), bf16[4,64,512]{2,1,0:T(8,128)(2,1)S(1)}, u32[]{:S(2)}, u32[]{:S(2)}) async-start(bf16[4,64,512]{2,1,0:T(8,128)(2,1)} %bitcast.5), calls=%async_computation | async-start | bytes 524288 | tf_op jit(solution)/shard_map/all_to_all | solution.py:311
  57.6 3.8 %collective-permute-start.10 = (bf16[256,1408]{1,0:T(8,128)(2,1)}, bf16[256,1408]{1,0:T(8,128)(2,1)}, u32[]{:S(2)}, u32[]{:S(2)}) collective-permute-start(bf16[256,1408]{1,0:T(8,128)(2,1)} %collective-permute-done.9), channel_id=1, source_target_pairs={{0,4},{8,0},{16,8},{24,16},{28,24},{20,28},{12,20},{4,12},{1,5},{9... | collective-permute-start | bytes 2162696 | tf_op jit(solution)/shard_map/ppermute | solution.py:262
  62.9 2.9 %broadcast.105.clone.1 = bf16[2048,1408]{1,0:T(8,128)(2,1)} broadcast(bf16[]{:T(256)} %constant.160.clone.1), dimensions={} | broadcast | bytes 5767170 | tf_op jit(solution)/shard_map/broadcast.9
  66.8 2.9 %broadcast.105.clone = bf16[2048,1408]{1,0:T(8,128)(2,1)} broadcast(bf16[]{:T(256)} %constant.160.clone.1), dimensions={} | broadcast | bytes 5767170 | tf_op jit(solution)/shard_map/broadcast.9
  70.9 8.7 %collective-permute-done.10 = bf16[256,1408]{1,0:T(8,128)(2,1)} collective-permute-done((bf16[256,1408]{1,0:T(8,128)(2,1)}, bf16[256,1408]{1,0:T(8,128)(2,1)}, u32[]{:S(2)}, u32[]{:S(2)}) %collective-permute-start.10) | collective-permute-done | bytes 720928 | tf_op jit(solution)/shard_map/ppermute | solution.py:262
  82.0 5.0 %fusion.26 = f32[64,2048]{1,0:T(8,128)S(1)} fusion(bf16[64,2048]{1,0:T(8,128)(2,1)S(1)} %bitcast.26, bf16[2048,2048]{1,0:T(8,128)(2,1)} %param.25), kind=kOutput, calls=%fused_computation.81 | convolution fusion | flops 536870912 | bytes 9175040 | tf_op jit(solution)/shard_map/dot_general | solution.py:315
  87.0 5.2 %multiply_reduce_fusion = (f32[64]{0:T(128)S(1)}, f32[64,2048]{1,0:T(8,128)S(1)}) fusion(f32[64,2048]{1,0:T(8,128)S(1)} %fusion.26, bf16[64,2048]{1,0:T(8,128)(2,1)S(1)} %bitcast.27, bf16[2048,2048]{1,0:T(8,128)(2,1)} %param.26, bf16[64,2048]{1,0:T(8,128)(2,1)S(1)} %copy-done.11), kind=kOutput, calls=%fused_computation.26 | convolution fusion | flops 538181568 | bytes 9961728 | tf_op jit(solution)/shard_map/dot_general | solution.py:316
  92.2 6.0 %collective-permute-done.11 = bf16[256,1408]{1,0:T(8,128)(2,1)} collective-permute-done((bf16[256,1408]{1,0:T(8,128)(2,1)}, bf16[256,1408]{1,0:T(8,128)(2,1)}, u32[]{:S(2)}, u32[]{:S(2)}) %collective-permute-start.11) | collective-permute-done | bytes 720928 | tf_op jit(solution)/shard_map/ppermute | solution.py:262
  104.6 12.6 %collective-permute-done.12 = bf16[256,1408]{1,0:T(8,128)(2,1)} collective-permute-done((bf16[256,1408]{1,0:T(8,128)(2,1)}, bf16[256,1408]{1,0:T(8,128)(2,1)}, u32[]{:S(2)}, u32[]{:S(2)}) %collective-permute-start.12) | collective-permute-done | bytes 720928 | tf_op jit(solution)/shard_map/ppermute | solution.py:262
  124.2 9.6 %collective-permute-done.13 = bf16[256,1408]{1,0:T(8,128)(2,1)S(1)} collective-permute-done((bf16[256,1408]{1,0:T(8,128)(2,1)}, bf16[256,1408]{1,0:T(8,128)(2,1)S(1)}, u32[]{:S(2)}, u32[]{:S(2)}) %collective-permute-start.13) | collective-permute-done | bytes 720928 | tf_op jit(solution)/shard_map/ppermute | solution.py:262
  141.9 7.5 %collective-permute-done.14 = bf16[256,1408]{1,0:T(8,128)(2,1)S(1)} collective-permute-done((bf16[256,1408]{1,0:T(8,128)(2,1)S(1)}, bf16[256,1408]{1,0:T(8,128)(2,1)S(1)}, u32[]{:S(2)}, u32[]{:S(2)}) %collective-permute-start.14) | collective-permute-done | bytes 720928 | tf_op jit(solution)/shard_map/ppermute | solution.py:262
  156.5 3.2 %collective-permute-done.15 = bf16[704,256]{1,0:T(8,128)(2,1)S(1)} collective-permute-done((bf16[704,256]{1,0:T(8,128)(2,1)S(1)}, bf16[704,256]{1,0:T(8,128)(2,1)S(1)}, u32[]{:S(2)}, u32[]{:S(2)}) %collective-permute-start.15) | collective-permute-done | bytes 360480 | tf_op jit(solution)/shard_map/ppermute | solution.py:262
  165.0 4.8 %collective-permute-done.16 = bf16[704,256]{1,0:T(8,128)(2,1)S(1)} collective-permute-done((bf16[704,256]{1,0:T(8,128)(2,1)S(1)}, bf16[704,256]{1,0:T(8,128)(2,1)S(1)}, u32[]{:S(2)}, u32[]{:S(2)}) %collective-permute-start.16) | collective-permute-done | bytes 360480 | tf_op jit(solution)/shard_map/ppermute | solution.py:262
  174.5 7.2 %collective-permute-done.17 = bf16[704,256]{1,0:T(8,128)(2,1)} collective-permute-done((bf16[704,256]{1,0:T(8,128)(2,1)S(1)}, bf16[704,256]{1,0:T(8,128)(2,1)}, u32[]{:S(2)}, u32[]{:S(2)}) %collective-permute-start.17) | collective-permute-done | bytes 360480 | tf_op jit(solution)/shard_map/ppermute | solution.py:262
  184.0 4.8 %fusion.27 = f32[256,1408]{1,0:T(8,128)S(1)} fusion(bf16[256,2048]{1,0:T(8,128)(2,1)} %all-gather.2.cloned.1.call-done, bf16[2048,1408]{1,0:T(8,128)(2,1)} %constant_dynamic-update-slice_fusion.16), kind=kOutput, calls=%fused_computation.82 | convolution fusion | flops 1476395008 | bytes 8257536 | tf_op jit(solution)/shard_map/dot_general | solution.py:323
  188.9 4.1 %collective-permute-start.7 = (f32[2,1408]{1,0:T(2,128)S(1)}, f32[2,1408]{1,0:T(2,128)S(1)}, u32[]{:S(2)}, u32[]{:S(2)}) collective-permute-start(f32[2,1408]{1,0:T(2,128)S(1)} %slice.32), channel_id=1, source_target_pairs={{0,4},{4,8},{8,12},{12,16},{16,20},{20,24},{24,28},{1,5},{5,9},{9,... | collective-permute-start | bytes 33800 | tf_op jit(solution)/shard_map/ppermute | solution.py:268
  196.0 3.2 %broadcast_in_dim.63 = bf16[1408,2048]{1,0:T(8,128)(2,1)} broadcast(bf16[]{:T(256)} %constant.160.clone.1), dimensions={} | broadcast | bytes 5767170 | tf_op jit(solution)/shard_map/broadcast_in_dim | solution.py:296
  207.5 2.6 collective-permute-done.20
  224.8 10.9 %convolution_convert_fusion = bf16[256,2048]{1,0:T(8,128)(2,1)} fusion(bf16[1408,2048]{1,0:T(8,128)(2,1)} %constant_dynamic-update-slice_fusion.24, f32[256,1408]{1,0:T(8,128)} %copy-done.13, f32[2,1408]{1,0:T(2,128)S(1)} %collective-permute-done.7, f32[1408]{0:T(1024)S(1)} %get-tuple-element.11, f32[1408]{0:T(1024)S(1)} %get-tuple-element.10, ...), kind=kOutput, calls=%fused_computation.2 | convolution fusion | flops 2958000128 | bytes 15101440 | tf_op jit(solution)/shard_map/dot_general | solution.py:333
  235.7 25.9 %reduce-scatter.2.cloned.1.call-done = bf16[64,2048]{1,0:T(8,128)(2,1)} async-done(((bf16[256,2048]{1,0:T(8,128)(2,1)}), bf16[64,2048]{1,0:T(8,128)(2,1)}) %reduce-scatter.2.cloned.1.call-update) | async-done | bytes 262160 | tf_op jit(solution)/shard_map/reduce_scatter | solution.py:334
  (142 shorter events, 88.3 us)
Async XLA Ops:
  6.5 20.7 %collective-permute-start.8 = (bf16[256,1408]{1,0:T(8,128)(2,1)}, bf16[256,1408]{1,0:T(8,128)(2,1)}, u32[]{:S(2)}, u32[]{:S(2)}) collective-permute-start(bf16[256,1408]{1,0:T(8,128)(2,1)} %param.30), channel_id=1, source_target_pairs={{0,4},{8,0},{16,8},{24,16},{28,24},{20,28},{12,20},{4,12},{1,5},{9... | collective-permute-start | bytes 2162696 | tf_op jit(solution)/shard_map/ppermute | solution.py:262
  9.5 19.7 %collective-permute-start = (bf16[256,1408]{1,0:T(8,128)(2,1)}, bf16[256,1408]{1,0:T(8,128)(2,1)S(1)}, u32[]{:S(2)}, u32[]{:S(2)}) collective-permute-start(bf16[256,1408]{1,0:T(8,128)(2,1)} %param.29), channel_id=1, source_target_pairs={{0,8},{8,16},{16,24},{24,28},{28,20},{20,12},{12,4},{4,0},{1,9},{9... | collective-permute-start | bytes 2162696 | tf_op jit(solution)/shard_map/ppermute | solution.py:262
  27.2 30.4 %collective-permute-start.9 = (bf16[256,1408]{1,0:T(8,128)(2,1)}, bf16[256,1408]{1,0:T(8,128)(2,1)}, u32[]{:S(2)}, u32[]{:S(2)}) collective-permute-start(bf16[256,1408]{1,0:T(8,128)(2,1)} %collective-permute-done.8), channel_id=1, source_target_pairs={{0,4},{8,0},{16,8},{24,16},{28,24},{20,28},{12,20},{4,12},{1,5},{9... | collective-permute-start | bytes 2162696 | tf_op jit(solution)/shard_map/ppermute | solution.py:262
  29.2 32.1 %collective-permute-start.1 = (bf16[256,1408]{1,0:T(8,128)(2,1)S(1)}, bf16[256,1408]{1,0:T(8,128)(2,1)}, u32[]{:S(2)}, u32[]{:S(2)}) collective-permute-start(bf16[256,1408]{1,0:T(8,128)(2,1)S(1)} %collective-permute-done), channel_id=1, source_target_pairs={{0,8},{8,16},{16,24},{24,28},{28,20},{20,12},{12,4},{4,0},{1,9},{9... | collective-permute-start | bytes 2162696 | tf_op jit(solution)/shard_map/ppermute | solution.py:262
  52.6 18.1 %all-to-all-start = ((bf16[4,64,512]{2,1,0:T(8,128)(2,1)}), bf16[4,64,512]{2,1,0:T(8,128)(2,1)S(1)}, u32[]{:S(2)}, u32[]{:S(2)}) async-start(bf16[4,64,512]{2,1,0:T(8,128)(2,1)} %bitcast.5), calls=%async_computation | async-start | bytes 524288 | tf_op jit(solution)/shard_map/all_to_all | solution.py:311
  56.2 127.9 %all-gather.2.cloned.1.call-start = ((), (), s32[]{:S(2)}) async-start(), calls=%async_computation.2 | async-start | bytes 1310720 | tf_op jit(solution)/shard_map/all_gather | solution.py:322
  57.6 22.0 %collective-permute-start.10 = (bf16[256,1408]{1,0:T(8,128)(2,1)}, bf16[256,1408]{1,0:T(8,128)(2,1)}, u32[]{:S(2)}, u32[]{:S(2)}) collective-permute-start(bf16[256,1408]{1,0:T(8,128)(2,1)} %collective-permute-done.9), channel_id=1, source_target_pairs={{0,4},{8,0},{16,8},{24,16},{28,24},{20,28},{12,20},{4,12},{1,5},{9... | collective-permute-start | bytes 2162696 | tf_op jit(solution)/shard_map/ppermute | solution.py:262
  61.3 18.9 %collective-permute-start.2 = (bf16[256,1408]{1,0:T(8,128)(2,1)}, bf16[256,1408]{1,0:T(8,128)(2,1)}, u32[]{:S(2)}, u32[]{:S(2)}) collective-permute-start(bf16[256,1408]{1,0:T(8,128)(2,1)} %collective-permute-done.1), channel_id=1, source_target_pairs={{0,8},{8,16},{16,24},{24,28},{28,20},{20,12},{12,4},{4,0},{1,9},{9... | collective-permute-start | bytes 2162696 | tf_op jit(solution)/shard_map/ppermute | solution.py:262
  79.6 18.6 %collective-permute-start.11 = (bf16[256,1408]{1,0:T(8,128)(2,1)}, bf16[256,1408]{1,0:T(8,128)(2,1)}, u32[]{:S(2)}, u32[]{:S(2)}) collective-permute-start(bf16[256,1408]{1,0:T(8,128)(2,1)} %collective-permute-done.10), channel_id=1, source_target_pairs={{0,4},{8,0},{16,8},{24,16},{28,24},{20,28},{12,20},{4,12},{1,5},{9... | collective-permute-start | bytes 2162696 | tf_op jit(solution)/shard_map/ppermute | solution.py:262
  80.2 19.4 %collective-permute-start.3 = (bf16[256,1408]{1,0:T(8,128)(2,1)}, bf16[256,1408]{1,0:T(8,128)(2,1)S(1)}, u32[]{:S(2)}, u32[]{:S(2)}) collective-permute-start(bf16[256,1408]{1,0:T(8,128)(2,1)} %collective-permute-done.2), channel_id=1, source_target_pairs={{0,8},{8,16},{16,24},{24,28},{28,20},{20,12},{12,4},{4,0},{1,9},{9... | collective-permute-start | bytes 2162696 | tf_op jit(solution)/shard_map/ppermute | solution.py:262
  98.2 19.0 %collective-permute-start.12 = (bf16[256,1408]{1,0:T(8,128)(2,1)}, bf16[256,1408]{1,0:T(8,128)(2,1)}, u32[]{:S(2)}, u32[]{:S(2)}) collective-permute-start(bf16[256,1408]{1,0:T(8,128)(2,1)} %collective-permute-done.11), channel_id=1, source_target_pairs={{0,4},{8,0},{16,8},{24,16},{28,24},{20,28},{12,20},{4,12},{1,5},{9... | collective-permute-start | bytes 2162696 | tf_op jit(solution)/shard_map/ppermute | solution.py:262
  99.6 17.5 %collective-permute-start.4 = (bf16[256,1408]{1,0:T(8,128)(2,1)S(1)}, bf16[256,1408]{1,0:T(8,128)(2,1)}, u32[]{:S(2)}, u32[]{:S(2)}) collective-permute-start(bf16[256,1408]{1,0:T(8,128)(2,1)S(1)} %collective-permute-done.3), channel_id=1, source_target_pairs={{0,8},{8,16},{16,24},{24,28},{28,20},{20,12},{12,4},{4,0},{1,9},{9... | collective-permute-start | bytes 2162696 | tf_op jit(solution)/shard_map/ppermute | solution.py:262
  102.5 159.1 %reduce-scatter.2.cloned.1.call-start = ((), (), s32[]{:S(2)}) async-start(), calls=%async_computation.3 | async-start | bytes 1310720 | tf_op jit(solution)/shard_map/reduce_scatter | solution.py:334
  117.2 16.7 %collective-permute-start.13 = (bf16[256,1408]{1,0:T(8,128)(2,1)}, bf16[256,1408]{1,0:T(8,128)(2,1)S(1)}, u32[]{:S(2)}, u32[]{:S(2)}) collective-permute-start(bf16[256,1408]{1,0:T(8,128)(2,1)} %collective-permute-done.12), channel_id=1, source_target_pairs={{0,4},{8,0},{16,8},{24,16},{28,24},{20,28},{12,20},{4,12},{1,5},{9... | collective-permute-start | bytes 2162696 | tf_op jit(solution)/shard_map/ppermute | solution.py:262
  117.2 16.9 %collective-permute-start.5 = (bf16[256,1408]{1,0:T(8,128)(2,1)}, bf16[256,1408]{1,0:T(8,128)(2,1)S(1)}, u32[]{:S(2)}, u32[]{:S(2)}) collective-permute-start(bf16[256,1408]{1,0:T(8,128)(2,1)} %collective-permute-done.4), channel_id=1, source_target_pairs={{0,8},{8,16},{16,24},{24,28},{28,20},{20,12},{12,4},{4,0},{1,9},{9... | collective-permute-start | bytes 2162696 | tf_op jit(solution)/shard_map/ppermute | solution.py:262
  133.8 15.6 %collective-permute-start.14 = (bf16[256,1408]{1,0:T(8,128)(2,1)S(1)}, bf16[256,1408]{1,0:T(8,128)(2,1)S(1)}, u32[]{:S(2)}, u32[]{:S(2)}) collective-permute-start(bf16[256,1408]{1,0:T(8,128)(2,1)S(1)} %collective-permute-done.13), channel_id=1, source_target_pairs={{0,4},{8,0},{16,8},{24,16},{28,24},{20,28},{12,20},{4,12},{1,5},{9... | collective-permute-start | bytes 2162696 | tf_op jit(solution)/shard_map/ppermute | solution.py:262
  134.1 16.3 %collective-permute-start.6 = (bf16[256,1408]{1,0:T(8,128)(2,1)S(1)}, bf16[256,1408]{1,0:T(8,128)(2,1)S(1)}, u32[]{:S(2)}, u32[]{:S(2)}) collective-permute-start(bf16[256,1408]{1,0:T(8,128)(2,1)S(1)} %collective-permute-done.5), channel_id=1, source_target_pairs={{0,8},{8,16},{16,24},{24,28},{28,20},{20,12},{12,4},{4,0},{1,9},{9... | collective-permute-start | bytes 2162696 | tf_op jit(solution)/shard_map/ppermute | solution.py:262
  159.7 10.1 %collective-permute-start.16 = (bf16[704,256]{1,0:T(8,128)(2,1)S(1)}, bf16[704,256]{1,0:T(8,128)(2,1)S(1)}, u32[]{:S(2)}, u32[]{:S(2)}) collective-permute-start(bf16[704,256]{1,0:T(8,128)(2,1)S(1)} %collective-permute-done.15), channel_id=1, source_target_pairs={{0,8},{8,16},{16,24},{24,28},{28,20},{20,12},{12,4},{4,0},{1,9},{9... | collective-permute-start | bytes 1081352 | tf_op jit(solution)/shard_map/ppermute | solution.py:262
  162.0 10.7 %collective-permute-start.23 = (bf16[704,256]{1,0:T(8,128)(2,1)S(1)}, bf16[704,256]{1,0:T(8,128)(2,1)S(1)}, u32[]{:S(2)}, u32[]{:S(2)}) collective-permute-start(bf16[704,256]{1,0:T(8,128)(2,1)S(1)} %collective-permute-done.22), channel_id=1, source_target_pairs={{0,4},{8,0},{16,8},{24,16},{28,24},{20,28},{12,20},{4,12},{1,5},{9... | collective-permute-start | bytes 1081352 | tf_op jit(solution)/shard_map/ppermute | solution.py:262
  169.8 11.9 %collective-permute-start.17 = (bf16[704,256]{1,0:T(8,128)(2,1)S(1)}, bf16[704,256]{1,0:T(8,128)(2,1)}, u32[]{:S(2)}, u32[]{:S(2)}) collective-permute-start(bf16[704,256]{1,0:T(8,128)(2,1)S(1)} %collective-permute-done.16), channel_id=1, source_target_pairs={{0,8},{8,16},{16,24},{24,28},{28,20},{20,12},{12,4},{4,0},{1,9},{9... | collective-permute-start | bytes 1081352 | tf_op jit(solution)/shard_map/ppermute | solution.py:262
  172.7 11.1 %collective-permute-start.24 = (bf16[704,256]{1,0:T(8,128)(2,1)S(1)}, bf16[704,256]{1,0:T(8,128)(2,1)S(1)}, u32[]{:S(2)}, u32[]{:S(2)}) collective-permute-start(bf16[704,256]{1,0:T(8,128)(2,1)S(1)} %collective-permute-done.23), channel_id=1, source_target_pairs={{0,4},{8,0},{16,8},{24,16},{28,24},{20,28},{12,20},{4,12},{1,5},{9... | collective-permute-start | bytes 1081352 | tf_op jit(solution)/shard_map/ppermute | solution.py:262
  181.7 11.2 %collective-permute-start.18 = (bf16[704,256]{1,0:T(8,128)(2,1)}, bf16[704,256]{1,0:T(8,128)(2,1)}, u32[]{:S(2)}, u32[]{:S(2)}) collective-permute-start(bf16[704,256]{1,0:T(8,128)(2,1)} %collective-permute-done.17), channel_id=1, source_target_pairs={{0,8},{8,16},{16,24},{24,28},{28,20},{20,12},{12,4},{4,0},{1,9},{9... | collective-permute-start | bytes 1081352 | tf_op jit(solution)/shard_map/ppermute | solution.py:262
  183.8 11.8 %collective-permute-start.25 = (bf16[704,256]{1,0:T(8,128)(2,1)S(1)}, bf16[704,256]{1,0:T(8,128)(2,1)S(1)}, u32[]{:S(2)}, u32[]{:S(2)}) collective-permute-start(bf16[704,256]{1,0:T(8,128)(2,1)S(1)} %collective-permute-done.24), channel_id=1, source_target_pairs={{0,4},{8,0},{16,8},{24,16},{28,24},{20,28},{12,20},{4,12},{1,5},{9... | collective-permute-start | bytes 1081352 | tf_op jit(solution)/shard_map/ppermute | solution.py:262
  188.9 35.9 %collective-permute-start.7 = (f32[2,1408]{1,0:T(2,128)S(1)}, f32[2,1408]{1,0:T(2,128)S(1)}, u32[]{:S(2)}, u32[]{:S(2)}) collective-permute-start(f32[2,1408]{1,0:T(2,128)S(1)} %slice.32), channel_id=1, source_target_pairs={{0,4},{4,8},{8,12},{12,16},{16,20},{20,24},{24,28},{1,5},{5,9},{9,... | collective-permute-start | bytes 33800 | tf_op jit(solution)/shard_map/ppermute | solution.py:268
  (22 other events, 282.2 us)
Sparse Core Ops, SparseCore 0:
  102.6 17.8 all-gather.1
  235.8 25.7 reduce-scatter.1

commit v2 on v1

--- a/solution.py
+++ b/solution.py
@@ -7,6 +7,7 @@
 from jax.experimental import pallas as pl
 from jax.experimental.pallas import tpu as pltpu
 from jax.sharding import PartitionSpec as P
+
 
 LANES = 128
 SEGMENTS = 8
@@ -251,10 +252,13 @@
     return jnp.where(index % 2 == 0, index // 2, n - 1 - index // 2)
 
 
-def ring_steps(n, block, direction):
+def ring_steps(halves, n, block, direction):
     order = ring_tables(n)
-    route = [(order[i], order[(i + direction) % n]) for i in range(n)]
-    place = ring_position(n, lax.axis_index("sp"))
+    route = [
+        (side * n + order[i], side * n + order[(i + direction) % n])
+        for side in range(halves) for i in range(n)
+    ]
+    place = ring_position(n, lax.rem(lax.axis_index("sp"), n))
     for step in range(n):
         owner = ring_owner(n, lax.rem(place - direction * step + n * n, n))
         yield block, owner
@@ -262,10 +266,12 @@
             block = lax.ppermute(block, "sp", route)
 
 
-def shifted_2(block, axis, distance):
-    devices = range(lax.axis_size(axis))
-    route = [(i - distance, i) for i in devices if i - distance in devices]
-    return lax.ppermute(block, axis, route)
+def scatter_sum(partial, tp_count):
+    rows, width = partial.shape
+    pieces = lax.all_to_all(
+        partial.reshape(tp_count, rows // tp_count, width), "tp", split_axis=0, concat_axis=0, tiled=True
+    )
+    return jnp.sum(pieces.astype(jnp.float32), axis=0)
 
 
 def local(
@@ -280,25 +286,37 @@
     groups = input_map.shape[1]
     model = ffn_gate.shape[0] * n_sp
     hidden_width = ffn_gate.shape[1]
-
-    gate_full = jnp.zeros((model, hidden_width), ffn_gate.dtype)
-    up_full = jnp.zeros((model, hidden_width), ffn_up.dtype)
     depth = ffn_gate.shape[0]
-    for block, owner in ring_steps(n_sp, ffn_gate, 1):
-        gate_full = lax.dynamic_update_slice(gate_full, block, (owner * depth, 0))
-        last_gate = block
-    for block, owner in ring_steps(n_sp, ffn_up, -1):
-        up_full = lax.dynamic_update_slice(up_full, block, (owner * depth, 0))
-        last_up = block
+    wide = ffn_down.shape[1]
+    around = n_sp // 2
+    side = lax.axis_index("sp") // around
+    place = lax.rem(lax.axis_index("sp"), around)
+    swap = [(i, (i + around) % n_sp) for i in range(n_sp)]
     half = hidden_width // 2
-    top, bottom = ffn_down[:half], ffn_down[half:]
-    top, bottom, last_gate, last_up = lax.optimization_barrier((top, bottom, last_gate, last_up))
-    down_full = jnp.zeros((hidden_width, model), ffn_down.dtype)
-    wide = ffn_down.shape[1]
-    for block, owner in ring_steps(n_sp, top, 1):
-        down_full = lax.dynamic_update_slice(down_full, block, (0, owner * wide))
-    for block, owner in ring_steps(n_sp, bottom, -1):
-        down_full = lax.dynamic_update_slice(down_full, block, (half, owner * wide))
+    first = side == 0
+
+    def halves(left, right):
+        return jnp.where(first, left, right), jnp.where(first, right, left)
+
+    gate_own, gate_give = halves(ffn_gate[:, :half], ffn_gate[:, half:])
+    up_own, up_give = halves(ffn_up[:, :half], ffn_up[:, half:])
+    down_own, down_give = halves(ffn_down[:half], ffn_down[half:])
+    gate_got = lax.ppermute(gate_give, "sp", swap)
+    up_got = lax.ppermute(up_give, "sp", swap)
+    down_got = lax.ppermute(down_give, "sp", swap)
+
+    gate_full = jnp.zeros((model, half), ffn_gate.dtype)
+    up_full = jnp.zeros((model, half), ffn_up.dtype)
+    down_full = jnp.zeros((half, model), ffn_down.dtype)
+    own_base, got_base = side * around, (1 - side) * around
+    for base, gate_block, up_block in ((own_base, gate_own, up_own), (got_base, gate_got, up_got)):
+        for block, owner in ring_steps(2, around, gate_block, 1):
+            gate_full = lax.dynamic_update_slice(gate_full, block, ((base + owner) * depth, 0))
+        for block, owner in ring_steps(2, around, up_block, -1):
+            up_full = lax.dynamic_update_slice(up_full, block, ((base + owner) * depth, 0))
+    for base, down_block, way in ((own_base, down_own, 1), (got_base, down_got, -1)):
+        for block, owner in ring_steps(2, around, down_block, way):
+            down_full = lax.dynamic_update_slice(down_full, block, (0, (base + owner) * wide))
 
     activated = state_space(
         n_sp, mixer_input, step_log, forget_log,
@@ -319,22 +337,41 @@
     stream_wide = stream.astype(jnp.float32)
     scale = lax.rsqrt(jnp.mean(stream_wide * stream_wide, axis=1, keepdims=True) + 1e-06)
     normed = (stream_wide * scale * norm_gain.astype(jnp.float32)).astype(jnp.bfloat16)
-    whole_rows = lax.all_gather(normed, "tp", axis=0, tiled=True)
-    gate_pre = jnp.dot(whole_rows, gate_full, preferred_element_type=jnp.float32)
-    up_pre = jnp.dot(whole_rows, up_full, preferred_element_type=jnp.float32)
+    other = lax.ppermute(normed, "sp", swap)
+    rows_mine = lax.all_gather(normed, "tp", axis=0, tiled=True)
+    rows_other = lax.all_gather(other, "tp", axis=0, tiled=True)
+
     history = conv_taps.shape[0] - 1
-    boundary = shifted_2(gate_pre[positions - history :], "sp", 1)
-    extended = jnp.concatenate([boundary, gate_pre], axis=0)
-    tap_weights = lax.dynamic_slice_in_dim(conv_taps, tp_index * hidden_width, hidden_width, 1)
-    conv_gate = tap_weights[0] * extended[0:positions]
-    for offset in range(1, history + 1):
-        conv_gate = conv_gate + tap_weights[offset] * extended[offset : offset + positions]
-    hidden = (jax.nn.silu(conv_gate) * up_pre).astype(jnp.bfloat16)
-    partial_value = jnp.dot(hidden, down_full, preferred_element_type=jnp.float32)
-    ffn_out = lax.psum_scatter(
-        partial_value.astype(jnp.bfloat16), "tp", scatter_dimension=0, tiled=True
-    ).astype(jnp.float32)
-    return (stream_wide + ffn_out).astype(jnp.bfloat16)
+    taps = lax.dynamic_slice_in_dim(conv_taps, tp_index * hidden_width + side * half, half, 1)
+    gate_mine = jnp.dot(rows_mine, gate_full, preferred_element_type=jnp.float32)
+    gate_other = jnp.dot(rows_other, gate_full, preferred_element_type=jnp.float32)
+    tail_mine, tail_other = gate_mine[positions - history :], gate_other[positions - history :]
+    tails = jnp.stack(halves(tail_mine, tail_other))
+    onward = [
+        (s * around + i, s * around + (i + 1) % around) for s in range(2) for i in range(around)
+    ]
+    came = lax.ppermute(tails, "sp", onward)
+    opening = place == 0
+    early = jnp.where(opening, 0.0, came[0])
+    late = jnp.where(opening, came[0], came[1])
+    before_mine, before_other = halves(early, late)
+
+    def hidden_rows(rows, gate_pre, before):
+        up_pre = jnp.dot(rows, up_full, preferred_element_type=jnp.float32)
+        extended = jnp.concatenate([before, gate_pre], axis=0)
+        conv_gate = taps[0] * extended[0:positions]
+        for offset in range(1, history + 1):
+            conv_gate = conv_gate + taps[offset] * extended[offset : offset + positions]
+        return (jax.nn.silu(conv_gate) * up_pre).astype(jnp.bfloat16)
+
+    hidden_other = hidden_rows(rows_other, gate_other, before_other)
+    hidden_mine = hidden_rows(rows_mine, gate_mine, before_mine)
+    part_other = jnp.dot(hidden_other, down_full, preferred_element_type=jnp.float32).astype(jnp.bfloat16)
+    sum_other = scatter_sum(part_other, tp_count).astype(jnp.bfloat16)
+    sum_back = lax.ppermute(sum_other, "sp", swap)
+    part_mine = jnp.dot(hidden_mine, down_full, preferred_element_type=jnp.float32).astype(jnp.bfloat16)
+    sum_mine = scatter_sum(part_mine, tp_count)
+    return (stream_wide + sum_mine + sum_back.astype(jnp.float32)).astype(jnp.bfloat16)
 
 
 def solution(mesh):

time: 271 us -> 275 us (1.015)
  local copies, waits for them, and re-layouts: 60.7 us -> 42.3 us
  matrix products: 25.8 us -> 33.8 us
  other arithmetic: 9.34 us -> 15.3 us
  waiting for transfers between devices: 96.2 us -> 101 us
    ppermute x1 -> x6, waiting for transfers between devices: 0.01 us -> 44.8 us  [the longest x1 26 us: local(): up_got = lax.ppermute(up_give, 'sp', swap)]
    ppermute x28 -> x18, waiting for transfers between devices: 70.3 us -> 33.5 us  [ring_steps(): block = lax.ppermute(block, 'sp', route)]
    reduce_scatter x1 -> x0, waiting for transfers between devices: 25.9 us -> none  [local(): lax.psum_scatter(partial_value.astype(jnp.bfloat16), 'tp', scatter_dimens...]
    all_to_all x0 -> x2, waiting for transfers between devices: none -> 16.5 us  [scatter_sum(): lax.all_to_all(partial.reshape(tp_count, rows // tp_count, width), 'tp',...]
    dynamic_update_slice x32 -> x21, local copies, waits for them, and re-layouts: 39.6 us -> 23.2 us  [the longest x7 9.48 us: local(): lax.dynamic_update_slice(gate_full, block, ((base + owner) * depth, 0))]
    ppermute x28 -> x18, starting transfers between devices: 33.1 us -> 19 us  [ring_steps(): block = lax.ppermute(block, 'sp', route)]
    ppermute x1 -> x6, starting transfers between devices: 4.05 us -> 12.9 us  [the longest x1 6.85 us: local(): up_got = lax.ppermute(up_give, 'sp', swap)]
    dot_general x2 -> x4, matrix products: 15.7 us -> 23.6 us  [the longest x1 8.33 us: local(): jnp.dot(hidden_mine, down_full, preferred_element_type=jnp.float32)]
  transfers between devices with their start and end apart: 32 -> 29, of which waited for: 19 -> 15; matrix products, arithmetic and copies ran while one was open for 31% -> 19% of each run, Pallas kernels for 9% -> 0%
where the time goes in v2:
time: 275 us; the launch traced here: 274 us
  waiting for transfers between devices  101 us (37%)
  starting transfers between devices  42.8 us (16%)
  local copies, waits for them, and re-layouts  42.3 us (15%)
  matrix products  33.8 us (12%)
  Pallas kernels  24.7 us (9%)
  other arithmetic  15.3 us (6%)
  between operations  13.9 us (5%)
    ppermute x18, waiting for transfers between devices, ring_steps(): block = lax.ppermute(block, 'sp', route)  33.5 us
    ppermute x1, waiting for transfers between devices, local(): up_got = lax.ppermute(up_give, 'sp', swap)  26 us
    pallas_call x1, Pallas kernels, state_space(): pl.pallas_call(functools.partial(ssm_kernel, n_sp, groups, per_tile, tile...  24.7 us
    ppermute x18, starting transfers between devices, ring_steps(): block = lax.ppermute(block, 'sp', route)  19 us
    all_to_all x2, waiting for transfers between devices, scatter_sum(): lax.all_to_all(partial.reshape(tp_count, rows // tp_count, width), 'tp',...  16.5 us
    dynamic_update_slice x7, local copies, waits for them, and re-layouts, local(): lax.dynamic_update_slice(gate_full, block, ((base + owner) * depth, 0))  9.48 us
    dynamic_update_slice x7, local copies, waits for them, and re-layouts, local(): lax.dynamic_update_slice(up_full, block, ((base + owner) * depth, 0))  8.46 us
    dot_general x1, matrix products, local(): jnp.dot(hidden_mine, down_full, preferred_element_type=jnp.float32)  8.33 us
  transfers between devices with their start and end apart: 29, of which 15 were waited for; matrix products, arithmetic and copies ran while one was open for 19% of the time, Pallas kernels for 0%

profile of v2, /device:TPU:0, one launch (start us, length us, event | category | flops | bytes accessed | tf_op | source)
XLA Modules:
  0.0 273.6 jit_solution(6787083138131067261)
XLA Ops:
  17.2 4.4 %select_n.248.w_in_ref = bf16[16,128,256]{2,1,0:T(8,128)(2,1)S(1)} reshape(bf16[16,8,16,2,2,64]{5,4,3,2,1,0:T(2,128)(2,1)} %broadcast_select_fusion.1) | data formatting | bytes 2097152 | tf_op jit(solution)/shard_map/jit(_where)/select_n | solution.py:200
  22.4 24.7 %shard_map.163 = bf16[256,512]{1,0:T(8,128)(2,1)} custom-call(bf16[256,512]{1,0:T(8,128)(2,1)S(1)} %copy-done, f32[256,128]{1,0:T(8,128)S(1)} %copy-done.1, f32[256,128]{1,0:T(8,128)S(1)} %copy-done.2, f32[4,16,128]{2,1,0:T(8,128)S(1)} %pad_maximum_fusion.2.rate_ref, bf16[16,128,256]{2,1,0:T(8,128)(2,1)S(1)} %select_n.248.w_in_ref, ...), custom_call_target="tpu_custom_call" | custom-call | flops 60000002048 | bytes 4000000 | tf_op jit(solution)/shard_map/pallas_call | solution.py:210
  47.1 3.5 %all-to-all-start = ((bf16[4,64,512]{2,1,0:T(8,128)(2,1)}), bf16[4,64,512]{2,1,0:T(8,128)(2,1)S(1)}, u32[]{:S(2)}, u32[]{:S(2)}) async-start(bf16[4,64,512]{2,1,0:T(8,128)(2,1)} %bitcast.5), calls=%async_computation | async-start | bytes 524288 | tf_op jit(solution)/shard_map/all_to_all | solution.py:329
  50.6 6.0 %all-to-all-done = bf16[4,64,512]{2,1,0:T(8,128)(2,1)S(1)} async-done(((bf16[4,64,512]{2,1,0:T(8,128)(2,1)}), bf16[4,64,512]{2,1,0:T(8,128)(2,1)S(1)}, u32[]{:S(2)}, u32[]{:S(2)}) %all-to-all-start) | async-done | bytes 262176 | tf_op jit(solution)/shard_map/all_to_all | solution.py:329
  56.9 5.0 %fusion.39 = f32[64,2048]{1,0:T(8,128)S(1)} fusion(bf16[64,2048]{1,0:T(8,128)(2,1)S(1)} %bitcast.41, bf16[2048,2048]{1,0:T(8,128)(2,1)} %param.25), kind=kOutput, calls=%fused_computation.103 | convolution fusion | flops 536870912 | bytes 9175040 | tf_op jit(solution)/shard_map/dot_general | solution.py:333
  61.9 5.2 %multiply_reduce_fusion = (f32[64]{0:T(128)S(1)}, f32[64,2048]{1,0:T(8,128)S(1)}) fusion(f32[64,2048]{1,0:T(8,128)S(1)} %fusion.39, bf16[64,2048]{1,0:T(8,128)(2,1)S(1)} %bitcast.42, bf16[2048,2048]{1,0:T(8,128)(2,1)} %param.26, bf16[64,2048]{1,0:T(8,128)(2,1)S(1)} %copy-done.10), kind=kOutput, calls=%fused_computation.33 | convolution fusion | flops 538181568 | bytes 9961728 | tf_op jit(solution)/shard_map/dot_general | solution.py:334
  74.1 6.9 %collective-permute-start.12 = (bf16[256,704]{1,0:T(8,128)(2,1)S(1)}, bf16[256,704]{1,0:T(8,128)(2,1)S(1)}, u32[]{:S(2)}, u32[]{:S(2)}) collective-permute-start(bf16[256,704]{1,0:T(8,128)(2,1)S(1)} %get-tuple-element.19), channel_id=1, source_target_pairs={{0,16},{4,20},{8,24},{12,28},{16,0},{20,4},{24,8},{28,12},{1,17},{... | collective-permute-start | bytes 1081352 | tf_op jit(solution)/shard_map/ppermute | solution.py:305
  88.9 5.4 %collective-permute-done.9 = bf16[256,704]{1,0:T(8,128)(2,1)S(1)} collective-permute-done((bf16[256,704]{1,0:T(8,128)(2,1)S(1)}, bf16[256,704]{1,0:T(8,128)(2,1)S(1)}, u32[]{:S(2)}, u32[]{:S(2)}) %collective-permute-start.9) | collective-permute-done | bytes 360480 | tf_op jit(solution)/shard_map/ppermute | solution.py:266
  94.3 26.0 %collective-permute-done.12 = bf16[256,704]{1,0:T(8,128)(2,1)S(1)} collective-permute-done((bf16[256,704]{1,0:T(8,128)(2,1)S(1)}, bf16[256,704]{1,0:T(8,128)(2,1)S(1)}, u32[]{:S(2)}, u32[]{:S(2)}) %collective-permute-start.12) | collective-permute-done | bytes 360480 | tf_op jit(solution)/shard_map/ppermute | solution.py:305
  122.1 7.6 %collective-permute-done.3 = bf16[256,704]{1,0:T(8,128)(2,1)} collective-permute-done((bf16[256,704]{1,0:T(8,128)(2,1)}, bf16[256,704]{1,0:T(8,128)(2,1)}, u32[]{:S(2)}, u32[]{:S(2)}) %collective-permute-start.3) | collective-permute-done | bytes 360480 | tf_op jit(solution)/shard_map/ppermute | solution.py:304
  131.8 5.7 %collective-permute-done.19 = bf16[704,256]{1,0:T(8,128)(2,1)} collective-permute-done((bf16[704,256]{1,0:T(8,128)(2,1)}, bf16[704,256]{1,0:T(8,128)(2,1)}, u32[]{:S(2)}, u32[]{:S(2)}) %collective-permute-start.19) | collective-permute-done | bytes 360480 | tf_op jit(solution)/shard_map/ppermute | solution.py:306
  145.3 4.6 %collective-permute-done.10 = bf16[256,704]{1,0:T(8,128)(2,1)} collective-permute-done((bf16[256,704]{1,0:T(8,128)(2,1)}, bf16[256,704]{1,0:T(8,128)(2,1)}, u32[]{:S(2)}, u32[]{:S(2)}) %collective-permute-start.10) | collective-permute-done | bytes 360480 | tf_op jit(solution)/shard_map/ppermute | solution.py:266
  150.0 8.4 %collective-permute-done.13 = bf16[256,704]{1,0:T(8,128)(2,1)} collective-permute-done((bf16[256,704]{1,0:T(8,128)(2,1)}, bf16[256,704]{1,0:T(8,128)(2,1)}, u32[]{:S(2)}, u32[]{:S(2)}) %collective-permute-start.13) | collective-permute-done | bytes 360480 | tf_op jit(solution)/shard_map/ppermute | solution.py:266
  167.1 3.9 %collective-permute-start.2 = (bf16[256,704]{1,0:T(8,128)(2,1)}, bf16[256,704]{1,0:T(8,128)(2,1)S(1)}, u32[]{:S(2)}, u32[]{:S(2)}) collective-permute-start(bf16[256,704]{1,0:T(8,128)(2,1)} %collective-permute-done.1), channel_id=1, source_target_pairs={{0,8},{8,12},{12,4},{4,0},{16,24},{24,28},{28,20},{20,16},{1,9},{9... | collective-permute-start | bytes 1081352 | tf_op jit(solution)/shard_map/ppermute | solution.py:266
  174.4 8.4 %collective-permute-done.14 = bf16[256,704]{1,0:T(8,128)(2,1)S(1)} collective-permute-done((bf16[256,704]{1,0:T(8,128)(2,1)}, bf16[256,704]{1,0:T(8,128)(2,1)S(1)}, u32[]{:S(2)}, u32[]{:S(2)}) %collective-permute-start.14) | collective-permute-done | bytes 360480 | tf_op jit(solution)/shard_map/ppermute | solution.py:266
  201.0 4.4 %fusion.40 = f32[256,704]{0,1:T(8,128)} fusion(bf16[256,2048]{1,0:T(8,128)(2,1)} %all-gather.3.cloned.1.call-done, bf16[2048,704]{1,0:T(8,128)(2,1)} %constant_dynamic-update-slice_fusion.16), kind=kOutput, calls=%fused_computation.104 | convolution fusion | flops 738197504 | bytes 4653056 | tf_op jit(solution)/shard_map/dot_general | solution.py:346
  205.4 3.6 %fusion.41 = f32[256,704]{0,1:T(8,128)S(1)} fusion(bf16[256,2048]{1,0:T(8,128)(2,1)} %all-gather.5.cloned.1.call-done, bf16[2048,704]{1,0:T(8,128)(2,1)} %constant_dynamic-update-slice_fusion.16), kind=kOutput, calls=%fused_computation.105 | convolution fusion | flops 738197504 | bytes 4653056 | tf_op jit(solution)/shard_map/dot_general | solution.py:347
  220.9 7.3 %convolution_convert_fusion = bf16[256,2048]{1,0:T(8,128)(2,1)} fusion(bf16[704,2048]{1,0:T(8,128)(2,1)S(1)} %constant_dynamic-update-slice_fusion, f32[256,704]{0,1:T(8,128)} %copy-done.12, f32[2,704]{0,1:T(8,128)} %get-tuple-element.17, f32[704]{0:T(1024)S(1)} %get-tuple-element.7, f32[704]{0:T(1024)S(1)} %get-tuple-element.6, ...), kind=kOutput, calls=%fused_computation.2 | convolution fusion | flops 1479262208 | bytes 8599296 | tf_op jit(solution)/shard_map/dot_general | solution.py:369
  228.2 3.7 %all-to-all-start.2 = ((bf16[4,64,2048]{2,1,0:T(8,128)(2,1)}), bf16[4,64,2048]{2,1,0:T(8,128)(2,1)S(1)}, u32[]{:S(2)}, u32[]{:S(2)}) async-start(bf16[4,64,2048]{2,1,0:T(8,128)(2,1)} %bitcast.45), calls=%async_computation.2 | async-start | bytes 2097152 | tf_op jit(solution)/shard_map/all_to_all | solution.py:271
  231.9 8.3 %convolution_convert_fusion.1 = bf16[256,2048]{1,0:T(8,128)(2,1)} fusion(bf16[704,2048]{1,0:T(8,128)(2,1)} %copy-done.3, f32[256,704]{0,1:T(8,128)} %fusion.40, f32[2,704]{0,1:T(8,128)} %get-tuple-element.16, f32[704]{0:T(1024)S(1)} %get-tuple-element.7, f32[704]{0:T(1024)S(1)} %get-tuple-element.6, f32[704]{0:T(1024)S(1)} %get-tuple-element.5, ...), kind=kOutput, calls=%fused_computation.3 | convolution fusion | flops 1479262208 | bytes 8599296 | tf_op jit(solution)/shard_map/dot_general | solution.py:372
  240.3 5.8 %all-to-all-done.2 = bf16[4,64,2048]{2,1,0:T(8,128)(2,1)S(1)} async-done(((bf16[4,64,2048]{2,1,0:T(8,128)(2,1)}), bf16[4,64,2048]{2,1,0:T(8,128)(2,1)S(1)}, u32[]{:S(2)}, u32[]{:S(2)}) %all-to-all-start.2) | async-done | bytes 1048608 | tf_op jit(solution)/shard_map/all_to_all | solution.py:271
  246.1 3.5 %all-to-all-start.1 = ((bf16[4,64,2048]{2,1,0:T(8,128)(2,1)}), bf16[4,64,2048]{2,1,0:T(8,128)(2,1)S(1)}, u32[]{:S(2)}, u32[]{:S(2)}) async-start(bf16[4,64,2048]{2,1,0:T(8,128)(2,1)} %bitcast.44), calls=%async_computation.1 | async-start | bytes 2097152 | tf_op jit(solution)/shard_map/all_to_all | solution.py:271
  249.8 3.6 %collective-permute-start.23 = (bf16[64,2048]{1,0:T(8,128)(2,1)S(1)}, bf16[64,2048]{1,0:T(8,128)(2,1)S(1)}, u32[]{:S(2)}, u32[]{:S(2)}) collective-permute-start(bf16[64,2048]{1,0:T(8,128)(2,1)S(1)} %reduce_sum.32), channel_id=1, source_target_pairs={{0,16},{4,20},{8,24},{12,28},{16,0},{20,4},{24,8},{28,12},{1,17},{... | collective-permute-start | bytes 786440 | tf_op jit(solution)/shard_map/ppermute | solution.py:371
  253.4 10.6 %all-to-all-done.1 = bf16[4,64,2048]{2,1,0:T(8,128)(2,1)S(1)} async-done(((bf16[4,64,2048]{2,1,0:T(8,128)(2,1)}), bf16[4,64,2048]{2,1,0:T(8,128)(2,1)S(1)}, u32[]{:S(2)}, u32[]{:S(2)}) %all-to-all-start.1) | async-done | bytes 1048608 | tf_op jit(solution)/shard_map/all_to_all | solution.py:271
  (138 shorter events, 83.0 us)
Async XLA Ops:
  50.6 150.4 %all-gather.3.cloned.1.call-start = ((), (), s32[]{:S(2)}) async-start(), calls=%async_computation.3 | async-start | bytes 1310720 | tf_op jit(solution)/shard_map/all_gather | solution.py:341
  68.0 137.5 %all-gather.5.cloned.1.call-start = ((), (), s32[]{:S(2)}) async-start(), calls=%async_computation.4 | async-start | bytes 1310720 | tf_op jit(solution)/shard_map/all_gather | solution.py:342
  71.2 23.1 %collective-permute-start.9 = (bf16[256,704]{1,0:T(8,128)(2,1)S(1)}, bf16[256,704]{1,0:T(8,128)(2,1)S(1)}, u32[]{:S(2)}, u32[]{:S(2)}) collective-permute-start(bf16[256,704]{1,0:T(8,128)(2,1)S(1)} %get-tuple-element.11), channel_id=1, source_target_pairs={{0,4},{8,0},{12,8},{4,12},{16,20},{24,16},{28,24},{20,28},{1,5},{9... | collective-permute-start | bytes 1081352 | tf_op jit(solution)/shard_map/ppermute | solution.py:266
  74.1 46.2 %collective-permute-start.12 = (bf16[256,704]{1,0:T(8,128)(2,1)S(1)}, bf16[256,704]{1,0:T(8,128)(2,1)S(1)}, u32[]{:S(2)}, u32[]{:S(2)}) collective-permute-start(bf16[256,704]{1,0:T(8,128)(2,1)S(1)} %get-tuple-element.19), channel_id=1, source_target_pairs={{0,16},{4,20},{8,24},{12,28},{16,0},{20,4},{24,8},{28,12},{1,17},{... | collective-permute-start | bytes 1081352 | tf_op jit(solution)/shard_map/ppermute | solution.py:305
  84.2 37.9 %collective-permute-start = (bf16[256,704]{1,0:T(8,128)(2,1)}, bf16[256,704]{1,0:T(8,128)(2,1)}, u32[]{:S(2)}, u32[]{:S(2)}) collective-permute-start(bf16[256,704]{1,0:T(8,128)(2,1)} %get-tuple-element.9), channel_id=1, source_target_pairs={{0,8},{8,12},{12,4},{4,0},{16,24},{24,28},{28,20},{20,16},{1,9},{9... | collective-permute-start | bytes 1081352 | tf_op jit(solution)/shard_map/ppermute | solution.py:266
  85.5 44.3 %collective-permute-start.3 = (bf16[256,704]{1,0:T(8,128)(2,1)}, bf16[256,704]{1,0:T(8,128)(2,1)}, u32[]{:S(2)}, u32[]{:S(2)}) collective-permute-start(bf16[256,704]{1,0:T(8,128)(2,1)} %get-tuple-element.18), channel_id=1, source_target_pairs={{0,16},{4,20},{8,24},{12,28},{16,0},{20,4},{24,8},{28,12},{1,17},{... | collective-permute-start | bytes 1081352 | tf_op jit(solution)/shard_map/ppermute | solution.py:304
  86.9 42.9 %collective-permute-start.16 = (bf16[704,256]{1,0:T(8,128)(2,1)}, bf16[704,256]{1,0:T(8,128)(2,1)}, u32[]{:S(2)}, u32[]{:S(2)}) collective-permute-start(bf16[704,256]{1,0:T(8,128)(2,1)} %get-tuple-element.13), channel_id=1, source_target_pairs={{0,8},{8,12},{12,4},{4,0},{16,24},{24,28},{28,20},{20,16},{1,9},{9... | collective-permute-start | bytes 1081352 | tf_op jit(solution)/shard_map/ppermute | solution.py:266
  94.3 43.1 %collective-permute-start.19 = (bf16[704,256]{1,0:T(8,128)(2,1)}, bf16[704,256]{1,0:T(8,128)(2,1)}, u32[]{:S(2)}, u32[]{:S(2)}) collective-permute-start(bf16[704,256]{1,0:T(8,128)(2,1)} %get-tuple-element.20), channel_id=1, source_target_pairs={{0,16},{4,20},{8,24},{12,28},{16,0},{20,4},{24,8},{28,12},{1,17},{... | collective-permute-start | bytes 1081352 | tf_op jit(solution)/shard_map/ppermute | solution.py:306
  121.1 20.6 %collective-permute-start.7 = (bf16[64,2048]{1,0:T(8,128)(2,1)}, bf16[64,2048]{1,0:T(8,128)(2,1)}, u32[]{:S(2)}, u32[]{:S(2)}) collective-permute-start(bf16[64,2048]{1,0:T(8,128)(2,1)} %multiply_convert_fusion.2), channel_id=1, source_target_pairs={{0,16},{4,20},{8,24},{12,28},{16,0},{20,4},{24,8},{28,12},{1,17},{... | collective-permute-start | bytes 786440 | tf_op jit(solution)/shard_map/ppermute | solution.py:340
  122.1 27.9 %collective-permute-start.10 = (bf16[256,704]{1,0:T(8,128)(2,1)}, bf16[256,704]{1,0:T(8,128)(2,1)}, u32[]{:S(2)}, u32[]{:S(2)}) collective-permute-start(bf16[256,704]{1,0:T(8,128)(2,1)} %copy-done.9), channel_id=1, source_target_pairs={{0,4},{8,0},{12,8},{4,12},{16,20},{24,16},{28,24},{20,28},{1,5},{9... | collective-permute-start | bytes 1081352 | tf_op jit(solution)/shard_map/ppermute | solution.py:266
  129.8 28.6 %collective-permute-start.13 = (bf16[256,704]{1,0:T(8,128)(2,1)}, bf16[256,704]{1,0:T(8,128)(2,1)}, u32[]{:S(2)}, u32[]{:S(2)}) collective-permute-start(bf16[256,704]{1,0:T(8,128)(2,1)} %copy-done.7), channel_id=1, source_target_pairs={{0,4},{8,0},{12,8},{4,12},{16,20},{24,16},{28,24},{20,28},{1,5},{9... | collective-permute-start | bytes 1081352 | tf_op jit(solution)/shard_map/ppermute | solution.py:266
  129.8 28.6 %collective-permute-start.1 = (bf16[256,704]{1,0:T(8,128)(2,1)}, bf16[256,704]{1,0:T(8,128)(2,1)}, u32[]{:S(2)}, u32[]{:S(2)}) collective-permute-start(bf16[256,704]{1,0:T(8,128)(2,1)} %collective-permute-done), channel_id=1, source_target_pairs={{0,8},{8,12},{12,4},{4,0},{16,24},{24,28},{28,20},{20,16},{1,9},{9... | collective-permute-start | bytes 1081352 | tf_op jit(solution)/shard_map/ppermute | solution.py:266
  137.5 20.9 %collective-permute-start.4 = (bf16[256,704]{1,0:T(8,128)(2,1)}, bf16[256,704]{1,0:T(8,128)(2,1)}, u32[]{:S(2)}, u32[]{:S(2)}) collective-permute-start(bf16[256,704]{1,0:T(8,128)(2,1)} %collective-permute-done.3), channel_id=1, source_target_pairs={{0,8},{8,12},{12,4},{4,0},{16,24},{24,28},{28,20},{20,16},{1,9},{9... | collective-permute-start | bytes 1081352 | tf_op jit(solution)/shard_map/ppermute | solution.py:266
  141.7 20.5 %collective-permute-start.17 = (bf16[704,256]{1,0:T(8,128)(2,1)}, bf16[704,256]{1,0:T(8,128)(2,1)}, u32[]{:S(2)}, u32[]{:S(2)}) collective-permute-start(bf16[704,256]{1,0:T(8,128)(2,1)} %collective-permute-done.16), channel_id=1, source_target_pairs={{0,8},{8,12},{12,4},{4,0},{16,24},{24,28},{28,20},{20,16},{1,9},{9... | collective-permute-start | bytes 1081352 | tf_op jit(solution)/shard_map/ppermute | solution.py:266
  150.0 17.1 %collective-permute-start.20 = (bf16[704,256]{1,0:T(8,128)(2,1)}, bf16[704,256]{1,0:T(8,128)(2,1)S(1)}, u32[]{:S(2)}, u32[]{:S(2)}) collective-permute-start(bf16[704,256]{1,0:T(8,128)(2,1)} %collective-permute-done.19), channel_id=1, source_target_pairs={{0,4},{8,0},{12,8},{4,12},{16,20},{24,16},{28,24},{20,28},{1,5},{9... | collective-permute-start | bytes 1081352 | tf_op jit(solution)/shard_map/ppermute | solution.py:266
  158.4 24.5 %collective-permute-start.14 = (bf16[256,704]{1,0:T(8,128)(2,1)}, bf16[256,704]{1,0:T(8,128)(2,1)S(1)}, u32[]{:S(2)}, u32[]{:S(2)}) collective-permute-start(bf16[256,704]{1,0:T(8,128)(2,1)} %collective-permute-done.13), channel_id=1, source_target_pairs={{0,4},{8,0},{12,8},{4,12},{16,20},{24,16},{28,24},{20,28},{1,5},{9... | collective-permute-start | bytes 1081352 | tf_op jit(solution)/shard_map/ppermute | solution.py:266
  158.4 24.5 %collective-permute-start.5 = (bf16[256,704]{1,0:T(8,128)(2,1)}, bf16[256,704]{1,0:T(8,128)(2,1)S(1)}, u32[]{:S(2)}, u32[]{:S(2)}) collective-permute-start(bf16[256,704]{1,0:T(8,128)(2,1)} %collective-permute-done.4), channel_id=1, source_target_pairs={{0,8},{8,12},{12,4},{4,0},{16,24},{24,28},{28,20},{20,16},{1,9},{9... | collective-permute-start | bytes 1081352 | tf_op jit(solution)/shard_map/ppermute | solution.py:266
  162.2 23.4 %collective-permute-start.18 = (bf16[704,256]{1,0:T(8,128)(2,1)}, bf16[704,256]{1,0:T(8,128)(2,1)S(1)}, u32[]{:S(2)}, u32[]{:S(2)}) collective-permute-start(bf16[704,256]{1,0:T(8,128)(2,1)} %collective-permute-done.17), channel_id=1, source_target_pairs={{0,8},{8,12},{12,4},{4,0},{16,24},{24,28},{28,20},{20,16},{1,9},{9... | collective-permute-start | bytes 1081352 | tf_op jit(solution)/shard_map/ppermute | solution.py:266
  167.1 23.6 %collective-permute-start.2 = (bf16[256,704]{1,0:T(8,128)(2,1)}, bf16[256,704]{1,0:T(8,128)(2,1)S(1)}, u32[]{:S(2)}, u32[]{:S(2)}) collective-permute-start(bf16[256,704]{1,0:T(8,128)(2,1)} %collective-permute-done.1), channel_id=1, source_target_pairs={{0,8},{8,12},{12,4},{4,0},{16,24},{24,28},{28,20},{20,16},{1,9},{9... | collective-permute-start | bytes 1081352 | tf_op jit(solution)/shard_map/ppermute | solution.py:266
  182.9 16.6 %collective-permute-start.15 = (bf16[256,704]{1,0:T(8,128)(2,1)S(1)}, bf16[256,704]{1,0:T(8,128)(2,1)S(1)}, u32[]{:S(2)}, u32[]{:S(2)}) collective-permute-start(bf16[256,704]{1,0:T(8,128)(2,1)S(1)} %collective-permute-done.14), channel_id=1, source_target_pairs={{0,4},{8,0},{12,8},{4,12},{16,20},{24,16},{28,24},{20,28},{1,5},{9... | collective-permute-start | bytes 1081352 | tf_op jit(solution)/shard_map/ppermute | solution.py:266
  182.9 17.4 %collective-permute-start.6 = (bf16[256,704]{1,0:T(8,128)(2,1)S(1)}, bf16[256,704]{1,0:T(8,128)(2,1)S(1)}, u32[]{:S(2)}, u32[]{:S(2)}) collective-permute-start(bf16[256,704]{1,0:T(8,128)(2,1)S(1)} %collective-permute-done.5), channel_id=1, source_target_pairs={{0,8},{8,12},{12,4},{4,0},{16,24},{24,28},{28,20},{20,16},{1,9},{9... | collective-permute-start | bytes 1081352 | tf_op jit(solution)/shard_map/ppermute | solution.py:266
  190.7 24.2 %collective-permute-start.22 = (bf16[704,256]{1,0:T(8,128)(2,1)}, bf16[704,256]{1,0:T(8,128)(2,1)}, u32[]{:S(2)}, u32[]{:S(2)}) collective-permute-start(bf16[704,256]{1,0:T(8,128)(2,1)} %collective-permute-done.21), channel_id=1, source_target_pairs={{0,4},{8,0},{12,8},{4,12},{16,20},{24,16},{28,24},{20,28},{1,5},{9... | collective-permute-start | bytes 1081352 | tf_op jit(solution)/shard_map/ppermute | solution.py:266
  228.2 17.9 %all-to-all-start.2 = ((bf16[4,64,2048]{2,1,0:T(8,128)(2,1)}), bf16[4,64,2048]{2,1,0:T(8,128)(2,1)S(1)}, u32[]{:S(2)}, u32[]{:S(2)}) async-start(bf16[4,64,2048]{2,1,0:T(8,128)(2,1)} %bitcast.45), calls=%async_computation.2 | async-start | bytes 2097152 | tf_op jit(solution)/shard_map/all_to_all | solution.py:271
  246.1 17.9 %all-to-all-start.1 = ((bf16[4,64,2048]{2,1,0:T(8,128)(2,1)}), bf16[4,64,2048]{2,1,0:T(8,128)(2,1)S(1)}, u32[]{:S(2)}, u32[]{:S(2)}) async-start(bf16[4,64,2048]{2,1,0:T(8,128)(2,1)} %bitcast.44), calls=%async_computation.1 | async-start | bytes 2097152 | tf_op jit(solution)/shard_map/all_to_all | solution.py:271
  (19 other events, 224.0 us)
Sparse Core Ops, SparseCore 0:
  68.1 23.2 all-gather.2
  145.4 17.3 all-gather.4
